TPU v7x, 512 devices: a whole 4x4x16 slice. The times are simulated.
512 devices in a mesh: ep: 32 (over z, core), tp: 16 (over y, x).
Axes of the slice: x: 4, y: 4, z: 16, core: 2. Of those that a mesh axis runs over, the one named last changes fastest.
Arguments:
- outer_gate: bfloat16 [4096, 2048], P('ep', 'tp'), may hold values from -6 to 6
- inner_gate: bfloat16 [4096, 2048], P('ep', 'tp'), may hold values from -6 to 6
- conv_value: bfloat16 [4096, 2048], P('ep', 'tp'), may hold values from -6 to 6
- conv_taps: bfloat16 [3, 2048], P(None, 'tp'), may hold values from -3.5 to 3.5
- mix_out: bfloat16 [2048, 2048], P(None, 'tp')
- gain_mixer: bfloat16 [2048], P('tp'), may hold values from 0.099609375 to 1.8984375
- bias_mixer: bfloat16 [2048], P('tp'), may hold values from -3 to 3
- moe_input: bfloat16 [4096, 2048], P('ep'), may hold values from -6 to 6
- route_ids: int32 [4096, 4], P('ep'), may hold values from 0 to 31, all different within a row; in each aligned block of 128 rows (0 to 127, 128 to 255, ...) at most 24 rows name the same one
- route_weights: float32 [4096, 4], P('ep'), may hold values from 0.1 to 1.2
- expert_gate: bfloat16 [32, 2048, 2048], P('ep', None, 'tp'), may hold values from -0.125 to 0.125
- expert_up: bfloat16 [32, 2048, 2048], P('ep', None, 'tp'), may hold values from -0.125 to 0.125
- expert_down: bfloat16 [32, 2048, 2048], P('ep', None, 'tp')
- shared_gate: bfloat16 [2048, 2048], P(None, 'tp'), may hold values from -0.125 to 0.125
- shared_up: bfloat16 [2048, 2048], P(None, 'tp'), may hold values from -0.125 to 0.125
- shared_down: bfloat16 [2048, 2048], P(None, 'tp')
- gain_experts: bfloat16 [2048], P('tp'), may hold values from 0.099609375 to 1.8984375
- bias_experts: bfloat16 [2048], P('tp'), may hold values from -3 to 3
Outputs:
- out_mixer: bfloat16 [4096, 2048], P('ep', 'tp')
- out_experts: bfloat16 [4096, 2048], P('ep', 'tp')
Inputs may be any that keep to these rules, and one draw needn't show every extreme that they name: `route_ids`: each row names 4 different experts. Among the rows of one index of ep (aligned blocks of 128 rows) no expert is named more than 24 times, a bound that some block reaches.
All inputs are finite; a program needn't handle non-finite values.
Results may differ from a plain program's by a relative error of at most 0.0055.
Values may be sent and summed in bfloat16 or wider, within the bound.
No kernel may reach another device: no remote copies, remote signals or barrier semaphores. Data moves between devices by JAX's collectives and lax.ppermute only.
A program may use at most 64 MiB of HBM per device.

v0:
```python
import jax
import jax.numpy as jnp
from jax import lax
from jax.experimental import pallas as pl
from jax.experimental.pallas import tpu as pltpu
from jax.sharding import Mesh
from jax.sharding import PartitionSpec as P


SEQS = 1
F32 = jnp.float32
BF16 = jnp.bfloat16
TP = ("y", "x")
LIMIT = pltpu.CompilerParams(vmem_limit_bytes=20 * 2**20)


def shifted(block, axis, distance):
    devices = range(lax.axis_size(axis))
    route = [(i - distance, i) for i in devices if i - distance in devices]
    return lax.ppermute(block, axis, route)


def rotated(x, distance):
    count = lax.axis_size("y")
    return lax.ppermute(x, "y", [(i, (i + distance) % count) for i in range(count)])


def exchanged(x, axis):
    return lax.all_to_all(x, axis, split_axis=0, concat_axis=0, tiled=True)


def vmem(count):
    return [pl.BlockSpec(memory_space=pltpu.VMEM) for _ in range(count)]


def near(*arrays):
    return [pltpu.with_memory_space_constraint(a, pltpu.VMEM) for a in arrays]


def iota(shape, dim):
    return lax.broadcasted_iota(jnp.int32, shape, dim)


def chunk(index, size):
    return pl.ds(pl.multiple_of(index * size, size), size)


SLOTS, BLOCKS = 6, 4


def ordinals(ids):
    tokens = ids.shape[1]
    experts = iota((32, tokens), 0)
    named = jnp.zeros((32, tokens), F32)
    for k in range(ids.shape[0]):
        named = named + (ids[k : k + 1, :] == experts).astype(F32)
    before = (iota((tokens, tokens), 0) <= iota((tokens, tokens), 1)).astype(BF16)
    place = jnp.dot(named.astype(BF16), before, preferred_element_type=F32)
    return (named * place).astype(BF16), experts


def spread_over(code, rows, each):
    expert_of = (iota((rows, 32), 0) // each == iota((rows, 32), 1)).astype(BF16)
    return expert_of, jnp.dot(expert_of, code, preferred_element_type=F32)


def pack_kernel(ids_ref, x_hbm, gate_hbm, up_hbm, out_ref, stack_ref, x_ref, sems):
    moves = (
        pltpu.make_async_copy(x_hbm.at[:, chunk(lax.axis_index("x"), 512)], x_ref, sems.at[0]),
        pltpu.make_async_copy(gate_hbm.at[0], stack_ref.at[0], sems.at[1]),
        pltpu.make_async_copy(gate_hbm.at[1], stack_ref.at[1], sems.at[2]),
        pltpu.make_async_copy(up_hbm.at[0], stack_ref.at[2], sems.at[3]),
        pltpu.make_async_copy(up_hbm.at[1], stack_ref.at[3], sems.at[4]),
    )
    for move in moves:
        move.start()
    code, _ = ordinals(ids_ref[...])
    _, spread = spread_over(code, 32 * SLOTS * BLOCKS, SLOTS * BLOCKS)
    wanted = iota(spread.shape, 0) % (SLOTS * BLOCKS) // BLOCKS + (lax.axis_index("y") * SLOTS + 1)
    here = (spread == wanted.astype(F32)).astype(BF16)
    moves[0].wait()
    taken = jnp.dot(here, x_ref[...], preferred_element_type=F32)
    part = iota(out_ref.shape, 0) % BLOCKS
    out = taken[:, 0:128]
    for b in range(1, BLOCKS):
        out = jnp.where(part == b, taken[:, b * 128 : (b + 1) * 128], out)
    out_ref[...] = out.astype(BF16)
    for move in moves[1:]:
        move.wait()


def pack(ids, x, gate, up):
    anywhere = pl.BlockSpec(memory_space=pltpu.HBM)
    return pl.pallas_call(
        pack_kernel,
        name="pack",
        compiler_params=LIMIT,
        out_shape=[pltpu.VMEM((768, 128), BF16), pltpu.VMEM((4, 1024, 128), BF16)],
        in_specs=vmem(1) + [anywhere] * 3,
        out_specs=vmem(2),
        scratch_shapes=[pltpu.VMEM((128, 512), BF16), pltpu.SemaphoreType.DMA((5,))],
    )(ids, *(pltpu.with_memory_space_constraint(a, pltpu.HBM) for a in (x, gate, up)))


def copies_kernel(a_ref, b_ref, out_ref):
    for q in range(4):
        out_ref[q, 0:768, :] = a_ref[...]
        out_ref[q, 768:1024, :] = b_ref[...]


def copies(a, b):
    return pl.pallas_call(
        copies_kernel,
        name="copies",
        compiler_params=LIMIT,
        out_shape=pltpu.VMEM((4, 1024, 128), BF16),
        in_specs=vmem(2),
        out_specs=vmem(1)[0],
    )(*near(a, b))


def hidden_kernel(x_ref, gate_ref, up_ref, w1_ref, w2_ref, gate3_ref, up3_ref, out_ref, wide_ref, rows_ref):
    for q in range(4):
        wide_ref[...] = x_ref[q, 0:768, :].astype(F32)
        for b in range(4):
            rows_ref[:, (q * 4 + b) * 128 : (q * 4 + b + 1) * 128] = wide_ref[
                pl.ds(b, 192, stride=4), :
            ].astype(BF16)
    rows = rows_ref[...]
    pairs = (
        (gate_ref[0], up_ref[0]),
        (w1_ref[0:2].reshape(2048, 128), w1_ref[2:4].reshape(2048, 128)),
        (w2_ref[0:2].reshape(2048, 128), w2_ref[2:4].reshape(2048, 128)),
        (gate3_ref[...].reshape(2048, 128), up3_ref[...].reshape(2048, 128)),
    )
    for r, (gate_w, up_w) in enumerate(pairs):
        gate = jnp.dot(rows, gate_w, preferred_element_type=F32)
        up = jnp.dot(rows, up_w, preferred_element_type=F32)
        hidden = (gate / (1.0 + jnp.exp(-gate)) * up).astype(BF16)
        for q in range(4):
            out_ref[q, :, r * 128 : (r + 1) * 128] = hidden


def hidden_of(x, *weights):
    return pl.pallas_call(
        hidden_kernel,
        name="hidden",
        compiler_params=LIMIT,
        out_shape=pltpu.VMEM((4, 192, 512), BF16),
        in_specs=vmem(7),
        out_specs=vmem(1)[0],
        scratch_shapes=[pltpu.VMEM((768, 128), F32), pltpu.VMEM((192, 2048), BF16)],
    )(*near(x), *weights)


def held_by(r):
    return (lax.axis_index("y") + (0, 3, 1, 2)[r]) % 4


def down_kernel(h_ref, w0_ref, w1_ref, w2_ref, w3_ref, out_ref, rows_ref):
    for r in range(4):
        for q in range(4):
            rows_ref[:, (r * 4 + q) * 128 : (r * 4 + q + 1) * 128] = h_ref[
                q, :, r * 128 : (r + 1) * 128
            ]
    to, of = iota((256, 192), 0), iota((256, 192), 1)
    place = ((to // 8 == of // SLOTS) & (to % 8 == of % SLOTS)).astype(BF16)
    for b, w_ref in enumerate((w0_ref, w1_ref, w2_ref, w3_ref)):
        total = jnp.zeros((192, 128), F32)
        for r in range(4):
            total = total + jnp.dot(
                rows_ref[:, r * 512 : (r + 1) * 512],
                w_ref[0, chunk(held_by(r), 512), :],
                preferred_element_type=F32,
            )
        placed = jnp.dot(place, total.astype(BF16), preferred_element_type=F32)
        out_ref[:, held_by(b)] = placed.astype(BF16).reshape(32, 8, 128)


def down_of(h, *weights):
    return pl.pallas_call(
        down_kernel,
        name="down",
        compiler_params=LIMIT,
        out_shape=pltpu.VMEM((32, 4, 8, 128), BF16),
        in_specs=vmem(5),
        out_specs=vmem(1)[0],
        scratch_shapes=[pltpu.VMEM((192, 2048), BF16)],
    )(*near(h), *weights)


def wide_kernel(own_ref, n1_ref, n2_ref, n3_ref, mix_ref, shared_ref, mixed_ref, sum_ref):
    for half, (w_ref, out_ref) in enumerate(((mix_ref, mixed_ref), (shared_ref, sum_ref))):
        total = jnp.zeros((128, 128), F32)
        for r, ref in enumerate((own_ref, n1_ref, n2_ref, n3_ref)):
            start = half * 128
            for q in range(4):
                total = total + jnp.dot(
                    ref[q, start : start + 128, :],
                    w_ref[chunk(held_by(r) * 4 + q, 128), :],
                    preferred_element_type=F32,
                )
        out_ref[...] = total


def wide_products(own, n1, n2, n3, mix_out, shared_down):
    return pl.pallas_call(
        wide_kernel,
        name="wide",
        compiler_params=LIMIT,
        out_shape=[pltpu.VMEM((128, 128), F32)] * 2,
        in_specs=vmem(6),
        out_specs=vmem(2),
    )(*near(own, n1, n2, n3), mix_out, shared_down)


def combine_kernel(ids_ref, weights_ref, back_ref, shared_ref, mixed_ref, combined_ref, out_ref):
    ids = ids_ref[...]
    code, experts = ordinals(ids)
    weight = jnp.zeros(experts.shape, F32)
    for k in range(ids.shape[0]):
        weight = weight + jnp.where(ids[k : k + 1, :] == experts, weights_ref[k : k + 1, :], 0.0)
    expert_of, spread = spread_over(code, 1024, 32)
    row = iota(spread.shape, 0)
    wanted = row % 32 // 8 * SLOTS + row % 8 + 1
    here = (spread == wanted.astype(F32)) & (row % 8 < SLOTS)
    back = back_ref[...].reshape(1024, 128)
    pieces = []
    for _ in range(3):
        piece = weight.astype(BF16)
        weight = weight - piece.astype(F32)
        piece = jnp.dot(expert_of, piece, preferred_element_type=F32)
        pieces.append(jnp.where(here, piece, 0.0).astype(BF16))
    routed = jnp.zeros((128, 128), F32)
    for piece in reversed(pieces):
        routed = routed + lax.dot_general(
            piece, back, (((0,), (0,)), ((), ())), preferred_element_type=F32
        )
    combined = routed + shared_ref[...]
    combined_ref[...] = combined
    for place, values in ((0, mixed_ref[...]), (2, combined)):
        turned = values.T
        total = jnp.sum(turned, axis=0, keepdims=True)
        square = jnp.sum(turned * turned, axis=0, keepdims=True)
        for p in range(16):
            out_ref[p, place : place + 1, :] = total
            out_ref[p, place + 1 : place + 2, :] = square


def combine(ids, weights, back, shared, mixed):
    return pl.pallas_call(
        combine_kernel,
        name="combine",
        compiler_params=LIMIT,
        out_shape=[pltpu.VMEM((128, 128), F32), pltpu.VMEM((16, 4, 128), F32)],
        in_specs=vmem(5),
        out_specs=vmem(2),
    )(ids, weights, *near(back, shared, mixed))


def finish_kernel(stats_ref, mixed_ref, combined_ref, coef_ref, out_mixer_ref, out_experts_ref):
    totals = stats_ref[0]
    for p in range(1, 16):
        totals = totals + stats_ref[p]
    totals = totals / 2048.0
    for place, values_ref, out_ref in (
        (0, mixed_ref, out_mixer_ref),
        (2, combined_ref, out_experts_ref),
    ):
        average = totals[place : place + 1]
        spread = totals[place + 1 : place + 2] - average * average
        scale = lax.rsqrt(spread + 1e-05)
        average = jnp.broadcast_to(average, (128, 128)).T
        scale = jnp.broadcast_to(scale, (128, 128)).T
        scaled = (values_ref[...] - average) * scale
        out_ref[...] = (
            scaled * coef_ref[place : place + 1, :] + coef_ref[place + 1 : place + 2, :]
        ).astype(BF16)


def finish(stats, mixed, combined, coef):
    return pl.pallas_call(
        finish_kernel,
        name="finish",
        compiler_params=LIMIT,
        out_shape=[jax.ShapeDtypeStruct((128, 128), BF16)] * 2,
        in_specs=vmem(4),
        out_specs=vmem(2),
    )(*near(stats, mixed, combined), coef)


def on_device(
    outer_gate,
    inner_gate,
    conv_value,
    conv_taps,
    mix_out,
    gain_mixer,
    bias_mixer,
    moe_input,
    route_ids,
    route_weights,
    expert_gate,
    expert_up,
    expert_down,
    shared_gate,
    shared_up,
    shared_down,
    gain_experts,
    bias_experts,
):
    token_rows, column_count = outer_gate.shape
    ep_count = lax.axis_size("ep")
    taps_count = conv_taps.shape[0]
    ids = route_ids.T
    sent, own = pack(
        ids, moe_input, expert_gate.reshape(2, 1024, 128), expert_up.reshape(2, 1024, 128)
    )
    arrived = exchanged(sent.reshape(ep_count, 24, 128), "ep").reshape(768, 128)
    before, after = rotated(own, 1), rotated(own, -1)
    far_gate = before[0:2]
    far_up = after[2:4]
    gate3, up3 = rotated(far_gate, 1), rotated(far_up, -1)
    down1, down2 = rotated(expert_down, 1), rotated(expert_down, -1)
    down3 = rotated(expert_down, 2)

    product = (inner_gate.astype(F32) * conv_value.astype(F32)).astype(BF16)
    border = shifted(product[token_rows - (taps_count - 1) :], "ep", 1)
    extended = jnp.concatenate([border, product], axis=0).astype(F32)
    seq_length = token_rows * ep_count // SEQS
    places = (
        lax.axis_index("ep") * token_rows + jnp.arange(token_rows, dtype=jnp.int32)
    ) % seq_length
    convolved = jnp.zeros((token_rows, column_count), F32)
    for offset in range(taps_count):
        delay_rows = taps_count - 1 - offset
        delayed = extended[offset : offset + token_rows]
        kept_mask = (places >= delay_rows).astype(F32)[:, None]
        convolved = convolved + conv_taps[offset].astype(F32)[None, :] * delayed * kept_mask
    weighted_in = (outer_gate.astype(F32) * convolved).astype(BF16)
    shared_gate_value = jnp.dot(moe_input, shared_gate, preferred_element_type=F32)
    shared_up_value = jnp.dot(moe_input, shared_up, preferred_element_type=F32)
    shared_hidden = (jax.nn.silu(shared_gate_value) * shared_up_value).astype(BF16)
    both = jnp.concatenate([weighted_in, shared_hidden])
    rows = exchanged(copies(arrived, both), "x")
    wide = rows[:, 768:]
    mixed, shared_sum = wide_products(
        wide, rotated(wide, 1), rotated(wide, -1), rotated(wide, 2), mix_out, shared_down
    )
    hidden = hidden_of(rows, expert_gate, expert_up, before, after, gate3, up3)
    hidden = exchanged(hidden, "x")
    expert_out = down_of(hidden, expert_down, down1, down2, down3)
    back = exchanged(expert_out.reshape(ep_count * 4, 8, 128), ("ep", "y"))
    combined, stats = combine(ids, route_weights.T, back, shared_sum, mixed)
    stats = exchanged(stats, TP)
    coef = jnp.stack([gain_mixer, bias_mixer, gain_experts, bias_experts]).astype(F32)
    return tuple(finish(stats, mixed, combined, coef))


def solution(mesh):
    split = Mesh(mesh.devices.reshape(mesh.shape["ep"], 4, 4), ("ep", "y", "x"))
    placed = (
        P("ep", TP),
        P("ep", TP),
        P("ep", TP),
        P(None, TP),
        P(None, TP),
        P(TP),
        P(TP),
        P("ep", None),
        P("ep", None),
        P("ep", None),
        P("ep", None, TP),
        P("ep", None, TP),
        P("ep", None, TP),
        P(None, TP),
        P(None, TP),
        P(None, TP),
        P(TP),
        P(TP),
    )
    return jax.shard_map(
        on_device,
        mesh=split,
        in_specs=placed,
        out_specs=(P("ep", TP), P("ep", TP)),
        check_vma=False,
    )
```

profile of v0, /device:TPU:1, one launch (start us, length us, event | category | flops | bytes accessed | tf_op | source)
XLA Modules:
  0.0 165.2 jit_solution(17306699855690064300)
XLA Ops:
  3.8 4.0 %collective-permute-start.1 = (bf16[4,1024,128]{2,1,0:T(8,128)(2,1)}, bf16[4,1024,128]{2,1,0:T(8,128)(2,1)S(1)}, u32[]{:S(2)}, u32[]{:S(2)}) collective-permute-start(bf16[4,1024,128]{2,1,0:T(8,128)(2,1)} %get-tuple-element.9), channel_id=1, source_target_pairs={{0,4},{4,8},{8,12},{12,0},{1,5},{5,9},{9,13},{13,1},{2,6},{6,10},{... | collective-permute-start | bytes 3145736 | tf_op jit(solution)/shard_map/ppermute | solution.py:25
  7.9 3.4 %collective-permute-start.2 = (bf16[4,1024,128]{2,1,0:T(8,128)(2,1)}, bf16[4,1024,128]{2,1,0:T(8,128)(2,1)}, u32[]{:S(2)}, u32[]{:S(2)}) collective-permute-start(bf16[4,1024,128]{2,1,0:T(8,128)(2,1)} %get-tuple-element.9), channel_id=1, source_target_pairs={{0,12},{4,0},{8,4},{12,8},{1,13},{5,1},{9,5},{13,9},{2,14},{6,2},{... | collective-permute-start | bytes 3145736 | tf_op jit(solution)/shard_map/ppermute | solution.py:25
  11.3 16.4 %all-to-all-start = ((bf16[32,24,128]{2,1,0:T(8,128)(2,1)}), bf16[32,24,128]{2,1,0:T(8,128)(2,1)S(1)}, u32[]{:S(2)}, u32[]{:S(2)}) async-start(bf16[32,24,128]{2,1,0:T(8,128)(2,1)} %bitcast.4), calls=%async_computation | async-start | bytes 393216 | tf_op jit(solution)/shard_map/all_to_all | solution.py:29
  27.7 3.5 %collective-permute-start = (bf16[2,128]{1,0:T(2,128)(2,1)S(1)}, bf16[2,128]{1,0:T(2,128)(2,1)S(1)}, u32[]{:S(2)}, u32[]{:S(2)}) collective-permute-start(bf16[2,128]{1,0:T(2,128)(2,1)S(1)} %slice.40), channel_id=1, source_target_pairs={{0,16},{16,32},{32,48},{48,64},{64,80},{80,96},{96,112},{112,128},... | collective-permute-start | bytes 1544 | tf_op jit(solution)/shard_map/ppermute | solution.py:20
  34.0 12.3 %all-to-all-done = bf16[32,24,128]{2,1,0:T(8,128)(2,1)S(1)} async-done(((bf16[32,24,128]{2,1,0:T(8,128)(2,1)}), bf16[32,24,128]{2,1,0:T(8,128)(2,1)S(1)}, u32[]{:S(2)}, u32[]{:S(2)}) %all-to-all-start) | async-done | bytes 196640 | tf_op jit(solution)/shard_map/all_to_all | solution.py:29
  47.4 4.0 %all-to-all-start.1 = ((bf16[4,1024,128]{2,1,0:T(8,128)(2,1)}), bf16[4,1024,128]{2,1,0:T(8,128)(2,1)S(1)}, u32[]{:S(2)}, u32[]{:S(2)}) async-start(bf16[4,1024,128]{2,1,0:T(8,128)(2,1)} %copies.1), calls=%async_computation.1 | async-start | bytes 2097152 | tf_op jit(solution)/shard_map/all_to_all | solution.py:29
  56.3 4.5 %collective-permute-start.4 = (bf16[2,1024,128]{2,1,0:T(8,128)(2,1)}, bf16[2,1024,128]{2,1,0:T(8,128)(2,1)}, u32[]{:S(2)}, u32[]{:S(2)}) collective-permute-start(bf16[2,1024,128]{2,1,0:T(8,128)(2,1)} %slice.45), channel_id=1, source_target_pairs={{0,12},{4,0},{8,4},{12,8},{1,13},{5,1},{9,5},{13,9},{2,14},{6,2},{... | collective-permute-start | bytes 1572872 | tf_op jit(solution)/shard_map/ppermute | solution.py:25
  60.8 3.9 %all-to-all-done.1.x_ref = bf16[4,1024,128]{2,1,0:T(8,128)(2,1)S(1)} async-done(((bf16[4,1024,128]{2,1,0:T(8,128)(2,1)}), bf16[4,1024,128]{2,1,0:T(8,128)(2,1)S(1)}, u32[]{:S(2)}, u32[]{:S(2)}) %all-to-all-start.1) | async-done | bytes 1048608 | tf_op jit(solution)/shard_map/all_to_all | solution.py:29
  67.4 2.8 %collective-permute-done.4.up3_ref = bf16[2,1024,128]{2,1,0:T(8,128)(2,1)} collective-permute-done((bf16[2,1024,128]{2,1,0:T(8,128)(2,1)}, bf16[2,1024,128]{2,1,0:T(8,128)(2,1)}, u32[]{:S(2)}, u32[]{:S(2)}) %collective-permute-start.4) | collective-permute-done | bytes 524320 | tf_op jit(solution)/shard_map/ppermute | solution.py:25
  71.2 4.3 %hidden.1 = bf16[4,192,512]{2,1,0:T(8,128)(2,1)} custom-call(bf16[4,1024,128]{2,1,0:T(8,128)(2,1)S(1)} %all-to-all-done.1.x_ref, bf16[1,2048,128]{2,1,0:T(8,128)(2,1)S(1)} %copy-done.1, bf16[1,2048,128]{2,1,0:T(8,128)(2,1)S(1)} %copy-done.2, bf16[4,1024,128]{2,1,0:T(8,128)(2,1)S(1)} %collective-permute-done.1.w1_ref, ...), custom_call_target="tpu_custom_call" | custom-call | tf_op jit(solution)/shard_map/hidden/pallas_call | solution.py:145
  75.6 4.1 %all-to-all-start.2 = ((bf16[4,192,512]{2,1,0:T(8,128)(2,1)}), bf16[4,192,512]{2,1,0:T(8,128)(2,1)S(1)}, u32[]{:S(2)}, u32[]{:S(2)}) async-start(bf16[4,192,512]{2,1,0:T(8,128)(2,1)} %hidden.1), calls=%async_computation.2 | async-start | bytes 1572864 | tf_op jit(solution)/shard_map/all_to_all | solution.py:29
  79.7 2.8 %collective-permute-start.5 = (bf16[1,2048,128]{2,1,0:T(8,128)(2,1)S(1)}, bf16[1,2048,128]{2,1,0:T(8,128)(2,1)S(1)}, u32[]{:S(2)}, u32[]{:S(2)}) collective-permute-start(bf16[1,2048,128]{2,1,0:T(8,128)(2,1)S(1)} %copy-done.3), channel_id=1, source_target_pairs={{0,4},{4,8},{8,12},{12,0},{1,5},{5,9},{9,13},{13,1},{2,6},{6,10},{... | collective-permute-start | bytes 1572872 | tf_op jit(solution)/shard_map/ppermute | solution.py:25
  82.5 4.4 %collective-permute-start.6 = (bf16[1,2048,128]{2,1,0:T(8,128)(2,1)S(1)}, bf16[1,2048,128]{2,1,0:T(8,128)(2,1)S(1)}, u32[]{:S(2)}, u32[]{:S(2)}) collective-permute-start(bf16[1,2048,128]{2,1,0:T(8,128)(2,1)S(1)} %copy-done.3), channel_id=1, source_target_pairs={{0,12},{4,0},{8,4},{12,8},{1,13},{5,1},{9,5},{13,9},{2,14},{6,2},{... | collective-permute-start | bytes 1572872 | tf_op jit(solution)/shard_map/ppermute | solution.py:25
  86.9 3.1 %collective-permute-start.7 = (bf16[1,2048,128]{2,1,0:T(8,128)(2,1)S(1)}, bf16[1,2048,128]{2,1,0:T(8,128)(2,1)S(1)}, u32[]{:S(2)}, u32[]{:S(2)}) collective-permute-start(bf16[1,2048,128]{2,1,0:T(8,128)(2,1)S(1)} %copy-done.3), channel_id=1, source_target_pairs={{0,8},{4,12},{8,0},{12,4},{1,9},{5,13},{9,1},{13,5},{2,10},{6,14},... | collective-permute-start | bytes 1572872 | tf_op jit(solution)/shard_map/ppermute | solution.py:25
  90.0 3.7 %collective-permute-done.5.w1_ref = bf16[1,2048,128]{2,1,0:T(8,128)(2,1)S(1)} collective-permute-done((bf16[1,2048,128]{2,1,0:T(8,128)(2,1)S(1)}, bf16[1,2048,128]{2,1,0:T(8,128)(2,1)S(1)}, u32[]{:S(2)}, u32[]{:S(2)}) %collective-permute-start.5) | collective-permute-done | bytes 524320 | tf_op jit(solution)/shard_map/ppermute | solution.py:25
  96.5 9.3 %collective-permute-done.7.w3_ref = bf16[1,2048,128]{2,1,0:T(8,128)(2,1)S(1)} collective-permute-done((bf16[1,2048,128]{2,1,0:T(8,128)(2,1)S(1)}, bf16[1,2048,128]{2,1,0:T(8,128)(2,1)S(1)}, u32[]{:S(2)}, u32[]{:S(2)}) %collective-permute-start.7) | collective-permute-done | bytes 524320 | tf_op jit(solution)/shard_map/ppermute | solution.py:25
  111.2 15.3 %all-to-all-start.3 = ((bf16[128,8,128]{2,1,0:T(8,128)(2,1)}), bf16[128,8,128]{2,1,0:T(8,128)(2,1)S(1)}, u32[]{:S(2)}, u32[]{:S(2)}) async-start(bf16[128,8,128]{2,1,0:T(8,128)(2,1)} %bitcast.9), calls=%async_computation.3 | async-start | bytes 524288 | tf_op jit(solution)/shard_map/all_to_all | solution.py:29
  126.5 3.3 %collective-permute-start.8 = (bf16[4,256,128]{2,1,0:T(8,128)(2,1)S(1)}, bf16[4,256,128]{2,1,0:T(8,128)(2,1)S(1)}, u32[]{:S(2)}, u32[]{:S(2)}) collective-permute-start(bf16[4,256,128]{2,1,0:T(8,128)(2,1)S(1)} %slice.46.own_ref), channel_id=1, source_target_pairs={{0,4},{4,8},{8,12},{12,0},{1,5},{5,9},{9,13},{13,1},{2,6},{6,10},{... | collective-permute-start | bytes 786440 | tf_op jit(solution)/shard_map/ppermute | solution.py:25
  129.8 3.2 %collective-permute-start.9 = (bf16[4,256,128]{2,1,0:T(8,128)(2,1)S(1)}, bf16[4,256,128]{2,1,0:T(8,128)(2,1)S(1)}, u32[]{:S(2)}, u32[]{:S(2)}) collective-permute-start(bf16[4,256,128]{2,1,0:T(8,128)(2,1)S(1)} %slice.46.own_ref), channel_id=1, source_target_pairs={{0,12},{4,0},{8,4},{12,8},{1,13},{5,1},{9,5},{13,9},{2,14},{6,2},{... | collective-permute-start | bytes 786440 | tf_op jit(solution)/shard_map/ppermute | solution.py:25
  133.0 3.6 %collective-permute-start.10 = (bf16[4,256,128]{2,1,0:T(8,128)(2,1)S(1)}, bf16[4,256,128]{2,1,0:T(8,128)(2,1)S(1)}, u32[]{:S(2)}, u32[]{:S(2)}) collective-permute-start(bf16[4,256,128]{2,1,0:T(8,128)(2,1)S(1)} %slice.46.own_ref), channel_id=1, source_target_pairs={{0,8},{4,12},{8,0},{12,4},{1,9},{5,13},{9,1},{13,5},{2,10},{6,14},... | collective-permute-start | bytes 786440 | tf_op jit(solution)/shard_map/ppermute | solution.py:25
  140.3 5.9 %collective-permute-done.10.n3_ref = bf16[4,256,128]{2,1,0:T(8,128)(2,1)S(1)} collective-permute-done((bf16[4,256,128]{2,1,0:T(8,128)(2,1)S(1)}, bf16[4,256,128]{2,1,0:T(8,128)(2,1)S(1)}, u32[]{:S(2)}, u32[]{:S(2)}) %collective-permute-start.10) | collective-permute-done | bytes 262176 | tf_op jit(solution)/shard_map/ppermute | solution.py:25
  146.7 3.3 %all-to-all-done.3.back_ref = bf16[128,8,128]{2,1,0:T(8,128)(2,1)S(1)} async-done(((bf16[128,8,128]{2,1,0:T(8,128)(2,1)}), bf16[128,8,128]{2,1,0:T(8,128)(2,1)S(1)}, u32[]{:S(2)}, u32[]{:S(2)}) %all-to-all-start.3) | async-done | bytes 262176 | tf_op jit(solution)/shard_map/all_to_all | solution.py:29
  152.3 5.7 %all-to-all-start.4 = ((f32[16,4,128]{2,1,0:T(4,128)}), f32[16,4,128]{2,1,0:T(4,128)S(1)}, u32[]{:S(2)}, u32[]{:S(2)}) async-start(f32[16,4,128]{2,1,0:T(4,128)} %get-tuple-element.12), calls=%async_computation.4 | async-start | bytes 65536 | tf_op jit(solution)/shard_map/all_to_all | solution.py:29
  158.7 5.7 %all-to-all-done.4.stats_ref = f32[16,4,128]{2,1,0:T(4,128)S(1)} async-done(((f32[16,4,128]{2,1,0:T(4,128)}), f32[16,4,128]{2,1,0:T(4,128)S(1)}, u32[]{:S(2)}, u32[]{:S(2)}) %all-to-all-start.4) | async-done | bytes 32800 | tf_op jit(solution)/shard_map/all_to_all | solution.py:29
  (73 shorter events, 31.7 us)
Async XLA Ops:
  0.6 30.7 %copy-start = (bf16[2048,128]{1,0:T(8,128)(2,1)S(1)}, bf16[2048,128]{1,0:T(8,128)(2,1)}, u32[]{:S(2)}) copy-start(bf16[2048,128]{1,0:T(8,128)(2,1)} %param.31) | copy-start | bytes 1572868
  1.4 29.9 %copy-start.12 = (bf16[128,2048]{1,0:T(8,128)(2,1)S(1)}, bf16[128,2048]{1,0:T(8,128)(2,1)}, u32[]{:S(2)}) copy-start(bf16[128,2048]{1,0:T(8,128)(2,1)} %x_hbm.1) | copy-start | bytes 1572868
  3.8 47.6 %collective-permute-start.1 = (bf16[4,1024,128]{2,1,0:T(8,128)(2,1)}, bf16[4,1024,128]{2,1,0:T(8,128)(2,1)S(1)}, u32[]{:S(2)}, u32[]{:S(2)}) collective-permute-start(bf16[4,1024,128]{2,1,0:T(8,128)(2,1)} %get-tuple-element.9), channel_id=1, source_target_pairs={{0,4},{4,8},{8,12},{12,0},{1,5},{5,9},{9,13},{13,1},{2,6},{6,10},{... | collective-permute-start | bytes 3145736 | tf_op jit(solution)/shard_map/ppermute | solution.py:25
  7.9 46.5 %collective-permute-start.2 = (bf16[4,1024,128]{2,1,0:T(8,128)(2,1)}, bf16[4,1024,128]{2,1,0:T(8,128)(2,1)}, u32[]{:S(2)}, u32[]{:S(2)}) collective-permute-start(bf16[4,1024,128]{2,1,0:T(8,128)(2,1)} %get-tuple-element.9), channel_id=1, source_target_pairs={{0,12},{4,0},{8,4},{12,8},{1,13},{5,1},{9,5},{13,9},{2,14},{6,2},{... | collective-permute-start | bytes 3145736 | tf_op jit(solution)/shard_map/ppermute | solution.py:25
  11.2 16.5 %copy-start.13 = (bf16[128,128]{1,0:T(8,128)(2,1)S(1)}, bf16[128,128]{1,0:T(8,128)(2,1)}, u32[]{:S(2)}) copy-start(bf16[128,128]{1,0:T(8,128)(2,1)} %param.20) | copy-start | bytes 98308
  11.2 16.5 %copy-start.14 = (bf16[128,128]{1,0:T(8,128)(2,1)S(1)}, bf16[128,128]{1,0:T(8,128)(2,1)}, u32[]{:S(2)}) copy-start(bf16[128,128]{1,0:T(8,128)(2,1)} %param.19) | copy-start | bytes 98308
  11.3 35.0 %all-to-all-start = ((bf16[32,24,128]{2,1,0:T(8,128)(2,1)}), bf16[32,24,128]{2,1,0:T(8,128)(2,1)S(1)}, u32[]{:S(2)}, u32[]{:S(2)}) async-start(bf16[32,24,128]{2,1,0:T(8,128)(2,1)} %bitcast.4), calls=%async_computation | async-start | bytes 393216 | tf_op jit(solution)/shard_map/all_to_all | solution.py:29
  27.7 5.3 %collective-permute-start = (bf16[2,128]{1,0:T(2,128)(2,1)S(1)}, bf16[2,128]{1,0:T(2,128)(2,1)S(1)}, u32[]{:S(2)}, u32[]{:S(2)}) collective-permute-start(bf16[2,128]{1,0:T(2,128)(2,1)S(1)} %slice.40), channel_id=1, source_target_pairs={{0,16},{16,32},{32,48},{48,64},{64,80},{80,96},{96,112},{112,128},... | collective-permute-start | bytes 1544 | tf_op jit(solution)/shard_map/ppermute | solution.py:20
  47.4 17.3 %all-to-all-start.1 = ((bf16[4,1024,128]{2,1,0:T(8,128)(2,1)}), bf16[4,1024,128]{2,1,0:T(8,128)(2,1)S(1)}, u32[]{:S(2)}, u32[]{:S(2)}) async-start(bf16[4,1024,128]{2,1,0:T(8,128)(2,1)} %copies.1), calls=%async_computation.1 | async-start | bytes 2097152 | tf_op jit(solution)/shard_map/all_to_all | solution.py:29
  52.3 17.9 %copy-start.1 = (bf16[1,2048,128]{2,1,0:T(8,128)(2,1)S(1)}, bf16[1,2048,128]{2,1,0:T(8,128)(2,1)}, u32[]{:S(2)}) copy-start(bf16[1,2048,128]{2,1,0:T(8,128)(2,1)} %gate_ref.1) | copy-start | bytes 1572868
  52.3 15.1 %collective-permute-start.3 = (bf16[2,1024,128]{2,1,0:T(8,128)(2,1)}, bf16[2,1024,128]{2,1,0:T(8,128)(2,1)}, u32[]{:S(2)}, u32[]{:S(2)}) collective-permute-start(bf16[2,1024,128]{2,1,0:T(8,128)(2,1)} %slice.44), channel_id=1, source_target_pairs={{0,4},{4,8},{8,12},{12,0},{1,5},{5,9},{9,13},{13,1},{2,6},{6,10},{... | collective-permute-start | bytes 1572872 | tf_op jit(solution)/shard_map/ppermute | solution.py:25
  56.3 13.9 %collective-permute-start.4 = (bf16[2,1024,128]{2,1,0:T(8,128)(2,1)}, bf16[2,1024,128]{2,1,0:T(8,128)(2,1)}, u32[]{:S(2)}, u32[]{:S(2)}) collective-permute-start(bf16[2,1024,128]{2,1,0:T(8,128)(2,1)} %slice.45), channel_id=1, source_target_pairs={{0,12},{4,0},{8,4},{12,8},{1,13},{5,1},{9,5},{13,9},{2,14},{6,2},{... | collective-permute-start | bytes 1572872 | tf_op jit(solution)/shard_map/ppermute | solution.py:25
  75.6 31.1 %all-to-all-start.2 = ((bf16[4,192,512]{2,1,0:T(8,128)(2,1)}), bf16[4,192,512]{2,1,0:T(8,128)(2,1)S(1)}, u32[]{:S(2)}, u32[]{:S(2)}) async-start(bf16[4,192,512]{2,1,0:T(8,128)(2,1)} %hidden.1), calls=%async_computation.2 | async-start | bytes 1572864 | tf_op jit(solution)/shard_map/all_to_all | solution.py:29
  79.7 14.0 %collective-permute-start.5 = (bf16[1,2048,128]{2,1,0:T(8,128)(2,1)S(1)}, bf16[1,2048,128]{2,1,0:T(8,128)(2,1)S(1)}, u32[]{:S(2)}, u32[]{:S(2)}) collective-permute-start(bf16[1,2048,128]{2,1,0:T(8,128)(2,1)S(1)} %copy-done.3), channel_id=1, source_target_pairs={{0,4},{4,8},{8,12},{12,0},{1,5},{5,9},{9,13},{13,1},{2,6},{6,10},{... | collective-permute-start | bytes 1572872 | tf_op jit(solution)/shard_map/ppermute | solution.py:25
  82.5 13.2 %collective-permute-start.6 = (bf16[1,2048,128]{2,1,0:T(8,128)(2,1)S(1)}, bf16[1,2048,128]{2,1,0:T(8,128)(2,1)S(1)}, u32[]{:S(2)}, u32[]{:S(2)}) collective-permute-start(bf16[1,2048,128]{2,1,0:T(8,128)(2,1)S(1)} %copy-done.3), channel_id=1, source_target_pairs={{0,12},{4,0},{8,4},{12,8},{1,13},{5,1},{9,5},{13,9},{2,14},{6,2},{... | collective-permute-start | bytes 1572872 | tf_op jit(solution)/shard_map/ppermute | solution.py:25
  86.9 18.9 %collective-permute-start.7 = (bf16[1,2048,128]{2,1,0:T(8,128)(2,1)S(1)}, bf16[1,2048,128]{2,1,0:T(8,128)(2,1)S(1)}, u32[]{:S(2)}, u32[]{:S(2)}) collective-permute-start(bf16[1,2048,128]{2,1,0:T(8,128)(2,1)S(1)} %copy-done.3), channel_id=1, source_target_pairs={{0,8},{4,12},{8,0},{12,4},{1,9},{5,13},{9,1},{13,5},{2,10},{6,14},... | collective-permute-start | bytes 1572872 | tf_op jit(solution)/shard_map/ppermute | solution.py:25
  111.2 35.0 %copy-start.4 = (bf16[2048,128]{1,0:T(8,128)(2,1)S(1)}, bf16[2048,128]{1,0:T(8,128)(2,1)}, u32[]{:S(2)}) copy-start(bf16[2048,128]{1,0:T(8,128)(2,1)} %mix_ref.1) | copy-start | bytes 1572868
  111.2 35.0 %copy-start.5 = (bf16[2048,128]{1,0:T(8,128)(2,1)S(1)}, bf16[2048,128]{1,0:T(8,128)(2,1)}, u32[]{:S(2)}) copy-start(bf16[2048,128]{1,0:T(8,128)(2,1)} %shared_ref.1) | copy-start | bytes 1572868
  111.2 38.7 %all-to-all-start.3 = ((bf16[128,8,128]{2,1,0:T(8,128)(2,1)}), bf16[128,8,128]{2,1,0:T(8,128)(2,1)S(1)}, u32[]{:S(2)}, u32[]{:S(2)}) async-start(bf16[128,8,128]{2,1,0:T(8,128)(2,1)} %bitcast.9), calls=%async_computation.3 | async-start | bytes 524288 | tf_op jit(solution)/shard_map/all_to_all | solution.py:29
  126.5 11.5 %collective-permute-start.8 = (bf16[4,256,128]{2,1,0:T(8,128)(2,1)S(1)}, bf16[4,256,128]{2,1,0:T(8,128)(2,1)S(1)}, u32[]{:S(2)}, u32[]{:S(2)}) collective-permute-start(bf16[4,256,128]{2,1,0:T(8,128)(2,1)S(1)} %slice.46.own_ref), channel_id=1, source_target_pairs={{0,4},{4,8},{8,12},{12,0},{1,5},{5,9},{9,13},{13,1},{2,6},{6,10},{... | collective-permute-start | bytes 786440 | tf_op jit(solution)/shard_map/ppermute | solution.py:25
  129.8 10.5 %collective-permute-start.9 = (bf16[4,256,128]{2,1,0:T(8,128)(2,1)S(1)}, bf16[4,256,128]{2,1,0:T(8,128)(2,1)S(1)}, u32[]{:S(2)}, u32[]{:S(2)}) collective-permute-start(bf16[4,256,128]{2,1,0:T(8,128)(2,1)S(1)} %slice.46.own_ref), channel_id=1, source_target_pairs={{0,12},{4,0},{8,4},{12,8},{1,13},{5,1},{9,5},{13,9},{2,14},{6,2},{... | collective-permute-start | bytes 786440 | tf_op jit(solution)/shard_map/ppermute | solution.py:25
  133.0 13.2 %collective-permute-start.10 = (bf16[4,256,128]{2,1,0:T(8,128)(2,1)S(1)}, bf16[4,256,128]{2,1,0:T(8,128)(2,1)S(1)}, u32[]{:S(2)}, u32[]{:S(2)}) collective-permute-start(bf16[4,256,128]{2,1,0:T(8,128)(2,1)S(1)} %slice.46.own_ref), channel_id=1, source_target_pairs={{0,8},{4,12},{8,0},{12,4},{1,9},{5,13},{9,1},{13,5},{2,10},{6,14},... | collective-permute-start | bytes 786440 | tf_op jit(solution)/shard_map/ppermute | solution.py:25
  150.6 7.4 %copy-start.20 = (bf16[128]{0:T(256)(128)(2,1)S(1)}, bf16[128]{0:T(256)(128)(2,1)}, u32[]{:S(2)}) copy-start(bf16[128]{0:T(256)(128)(2,1)} %param.23) | copy-start | bytes 772
  152.3 12.2 %all-to-all-start.4 = ((f32[16,4,128]{2,1,0:T(4,128)}), f32[16,4,128]{2,1,0:T(4,128)S(1)}, u32[]{:S(2)}, u32[]{:S(2)}) async-start(f32[16,4,128]{2,1,0:T(4,128)} %get-tuple-element.12), calls=%async_computation.4 | async-start | bytes 65536 | tf_op jit(solution)/shard_map/all_to_all | solution.py:29
  (14 other events, 14.7 us)
where the time goes:
time: 166 us; the launch traced here: 165 us
  starting transfers between devices  83.4 us (50%)
  waiting for transfers between devices  55.4 us (33%)
  Pallas kernels  13.3 us (8%)
  local copies, waits for them, and re-layouts  11.4 us (7%)
    all_to_all x5, starting transfers between devices, exchanged(): return lax.all_to_all(x, axis, split_axis=0, concat_axis=0, tiled=True)  45.5 us
    ppermute x10, starting transfers between devices, rotated(): lax.ppermute(x, 'y', [(i, (i + distance) % count) for i in range(count)])  34.4 us
    ppermute x10, waiting for transfers between devices, rotated(): lax.ppermute(x, 'y', [(i, (i + distance) % count) for i in range(count)])  30.1 us
    all_to_all x5, waiting for transfers between devices, exchanged(): return lax.all_to_all(x, axis, split_axis=0, concat_axis=0, tiled=True)  25.3 us
    unnamed x44, local copies, waits for them, and re-layouts  8.69 us
    pallas_call x1, Pallas kernels, hidden_of(): pl.pallas_call(hidden_kernel, name='hidden', compiler_params=LIMIT, out_s...  4.35 us
    ppermute x1, starting transfers between devices, shifted(): return lax.ppermute(block, axis, route)  3.54 us
  transfers between devices with their start and end apart: 16, of which 12 were waited for; matrix products, arithmetic and copies ran while one was open for 2% of the time, Pallas kernels for 1%

commit v1 on v0

--- a/solution.py
+++ b/solution.py
@@ -7,7 +7,6 @@
 from jax.sharding import PartitionSpec as P
 
 
-SEQS = 1
 F32 = jnp.float32
 BF16 = jnp.bfloat16
 TP = ("y", "x")
@@ -64,78 +63,152 @@
     return expert_of, jnp.dot(expert_of, code, preferred_element_type=F32)
 
 
-def pack_kernel(ids_ref, x_hbm, gate_hbm, up_hbm, out_ref, stack_ref, x_ref, sems):
-    moves = (
-        pltpu.make_async_copy(x_hbm.at[:, chunk(lax.axis_index("x"), 512)], x_ref, sems.at[0]),
-        pltpu.make_async_copy(gate_hbm.at[0], stack_ref.at[0], sems.at[1]),
-        pltpu.make_async_copy(gate_hbm.at[1], stack_ref.at[1], sems.at[2]),
-        pltpu.make_async_copy(up_hbm.at[0], stack_ref.at[2], sems.at[3]),
-        pltpu.make_async_copy(up_hbm.at[1], stack_ref.at[3], sems.at[4]),
+def side_by_side(gate_hbm, up_hbm, stack_ref, sems):
+    return tuple(
+        pltpu.make_async_copy(
+            ref.at[half * 1024 : half * 1024 + 1024],
+            stack_ref.at[half * 1024 : half * 1024 + 1024, side * 128 : side * 128 + 128],
+            sems.at[2 * side + half],
+        )
+        for side, ref in enumerate((gate_hbm, up_hbm))
+        for half in range(2)
     )
+
+
+def far(*arrays):
+    return [pltpu.with_memory_space_constraint(a, pltpu.HBM) for a in arrays]
+
+
+def hbm(count):
+    return [pl.BlockSpec(memory_space=pltpu.HBM) for _ in range(count)]
+
+
+def pack_kernel(
+    ids_hbm, x_hbm, gate_hbm, up_hbm, out_ref, stack_ref, ids_ref, x_ref, first_sem, sem, sems
+):
+    first = pltpu.make_async_copy(ids_hbm, ids_ref, first_sem)
+    first.start()
+    mine = pltpu.make_async_copy(x_hbm.at[:, chunk(lax.axis_index("x"), 512)], x_ref, sem)
+    mine.start()
+    moves = side_by_side(gate_hbm, up_hbm, stack_ref, sems)
     for move in moves:
         move.start()
+    first.wait()
     code, _ = ordinals(ids_ref[...])
     _, spread = spread_over(code, 32 * SLOTS * BLOCKS, SLOTS * BLOCKS)
     wanted = iota(spread.shape, 0) % (SLOTS * BLOCKS) // BLOCKS + (lax.axis_index("y") * SLOTS + 1)
     here = (spread == wanted.astype(F32)).astype(BF16)
-    moves[0].wait()
+    mine.wait()
     taken = jnp.dot(here, x_ref[...], preferred_element_type=F32)
     part = iota(out_ref.shape, 0) % BLOCKS
     out = taken[:, 0:128]
     for b in range(1, BLOCKS):
         out = jnp.where(part == b, taken[:, b * 128 : (b + 1) * 128], out)
     out_ref[...] = out.astype(BF16)
-    for move in moves[1:]:
+    for move in moves:
         move.wait()
 
 
 def pack(ids, x, gate, up):
-    anywhere = pl.BlockSpec(memory_space=pltpu.HBM)
     return pl.pallas_call(
         pack_kernel,
         name="pack",
         compiler_params=LIMIT,
-        out_shape=[pltpu.VMEM((768, 128), BF16), pltpu.VMEM((4, 1024, 128), BF16)],
-        in_specs=vmem(1) + [anywhere] * 3,
+        out_shape=[pltpu.HBM((768, 128), BF16), pltpu.VMEM((2048, 256), BF16)],
+        in_specs=hbm(4),
         out_specs=vmem(2),
-        scratch_shapes=[pltpu.VMEM((128, 512), BF16), pltpu.SemaphoreType.DMA((5,))],
-    )(ids, *(pltpu.with_memory_space_constraint(a, pltpu.HBM) for a in (x, gate, up)))
-
-
-def copies_kernel(a_ref, b_ref, out_ref):
+        scratch_shapes=[
+            pltpu.VMEM((4, 128), jnp.int32),
+            pltpu.VMEM((128, 512), BF16),
+            pltpu.SemaphoreType.DMA(()),
+            pltpu.SemaphoreType.DMA(()),
+            pltpu.SemaphoreType.DMA((4,)),
+        ],
+    )(*far(ids, x, gate, up))
+
+
+def half_kernel(x_ref, out_ref):
+    out_ref[...] = x_ref[...]
+
+
+def half_of(x, place):
+    return pl.pallas_call(
+        half_kernel,
+        name="half",
+        compiler_params=LIMIT,
+        grid=(1,),
+        out_shape=pltpu.VMEM((1024, 256), BF16),
+        in_specs=[pl.BlockSpec((1024, 256), lambda i: (place, 0))],
+        out_specs=pl.BlockSpec((1024, 256), lambda i: (0, 0)),
+    )(x)
+
+
+def front_kernel(inner_ref, value_ref, x_ref, gate_ref, up_ref, product_ref, tail_ref, hidden_ref):
+    product = (inner_ref[...].astype(F32) * value_ref[...].astype(F32)).astype(BF16)
+    product_ref[...] = product
+    tail_ref[...] = product[126:128]
+    gate = jnp.dot(x_ref[...], gate_ref[...], preferred_element_type=F32)
+    up = jnp.dot(x_ref[...], up_ref[...], preferred_element_type=F32)
+    hidden_ref[...] = (gate / (1.0 + jnp.exp(-gate)) * up).astype(BF16)
+
+
+def front(*arrays):
+    return pl.pallas_call(
+        front_kernel,
+        name="front",
+        compiler_params=LIMIT,
+        out_shape=[
+            pltpu.VMEM((128, 128), BF16),
+            pltpu.VMEM((2, 128), BF16),
+            pltpu.VMEM((128, 128), BF16),
+        ],
+        in_specs=vmem(5),
+        out_specs=vmem(3),
+    )(*arrays)
+
+
+def copies_kernel(a_ref, border_ref, product_ref, outer_ref, taps_ref, shared_ref, out_ref, rows_ref):
+    rows_ref[6:8, :] = border_ref[...].astype(F32)
+    rows_ref[8:136, :] = product_ref[...].astype(F32)
+    convolved = jnp.zeros((128, 128), F32)
+    for tap in range(3):
+        convolved = convolved + taps_ref[tap : tap + 1, :].astype(F32) * rows_ref[6 + tap : 134 + tap, :]
+    weighted = (outer_ref[...].astype(F32) * convolved).astype(BF16)
     for q in range(4):
         out_ref[q, 0:768, :] = a_ref[...]
-        out_ref[q, 768:1024, :] = b_ref[...]
-
-
-def copies(a, b):
+        out_ref[q, 768:896, :] = weighted
+        out_ref[q, 896:1024, :] = shared_ref[...]
+
+
+def copies(arrived, border, product, outer, taps, shared):
     return pl.pallas_call(
         copies_kernel,
         name="copies",
         compiler_params=LIMIT,
-        out_shape=pltpu.VMEM((4, 1024, 128), BF16),
-        in_specs=vmem(2),
+        out_shape=pltpu.HBM((4, 1024, 128), BF16),
+        in_specs=vmem(6),
         out_specs=vmem(1)[0],
-    )(*near(a, b))
-
-
-def hidden_kernel(x_ref, gate_ref, up_ref, w1_ref, w2_ref, gate3_ref, up3_ref, out_ref, wide_ref, rows_ref):
+        scratch_shapes=[pltpu.VMEM((136, 128), F32)],
+    )(*near(arrived, border, product), outer, taps, *near(shared))
+
+
+def hidden_kernel(x_ref, own_ref, w1_ref, w2_ref, low_ref, high_ref, out_ref, rest_ref, wide_ref, rows_ref):
     for q in range(4):
         wide_ref[...] = x_ref[q, 0:768, :].astype(F32)
         for b in range(4):
             rows_ref[:, (q * 4 + b) * 128 : (q * 4 + b + 1) * 128] = wide_ref[
                 pl.ds(b, 192, stride=4), :
             ].astype(BF16)
-    rows = rows_ref[...]
-    pairs = (
-        (gate_ref[0], up_ref[0]),
-        (w1_ref[0:2].reshape(2048, 128), w1_ref[2:4].reshape(2048, 128)),
-        (w2_ref[0:2].reshape(2048, 128), w2_ref[2:4].reshape(2048, 128)),
-        (gate3_ref[...].reshape(2048, 128), up3_ref[...].reshape(2048, 128)),
-    )
-    for r, (gate_w, up_w) in enumerate(pairs):
-        gate = jnp.dot(rows, gate_w, preferred_element_type=F32)
-        up = jnp.dot(rows, up_w, preferred_element_type=F32)
+        rest_ref[q] = x_ref[q, 768:1024, :]
+    for r in range(4):
+        if r < 3:
+            ref = (own_ref, w1_ref, w2_ref)[r]
+            both = jnp.dot(rows_ref[...], ref[...], preferred_element_type=F32)
+        else:
+            both = jnp.dot(
+                rows_ref[:, 0:1024], low_ref[...], preferred_element_type=F32
+            ) + jnp.dot(rows_ref[:, 1024:2048], high_ref[...], preferred_element_type=F32)
+        gate, up = both[:, 0:128], both[:, 128:256]
         hidden = (gate / (1.0 + jnp.exp(-gate)) * up).astype(BF16)
         for q in range(4):
             out_ref[q, :, r * 128 : (r + 1) * 128] = hidden
@@ -146,9 +219,9 @@
         hidden_kernel,
         name="hidden",
         compiler_params=LIMIT,
-        out_shape=pltpu.VMEM((4, 192, 512), BF16),
-        in_specs=vmem(7),
-        out_specs=vmem(1)[0],
+        out_shape=[pltpu.HBM((4, 192, 512), BF16), pltpu.VMEM((4, 256, 128), BF16)],
+        in_specs=vmem(6),
+        out_specs=vmem(2),
         scratch_shapes=[pltpu.VMEM((768, 128), F32), pltpu.VMEM((192, 2048), BF16)],
     )(*near(x), *weights)
 
@@ -160,19 +233,11 @@
 def down_kernel(h_ref, w0_ref, w1_ref, w2_ref, w3_ref, out_ref, rows_ref):
     for r in range(4):
         for q in range(4):
-            rows_ref[:, (r * 4 + q) * 128 : (r * 4 + q + 1) * 128] = h_ref[
-                q, :, r * 128 : (r + 1) * 128
-            ]
+            rows_ref[:, chunk(held_by(r) * 4 + q, 128)] = h_ref[q, :, r * 128 : (r + 1) * 128]
     to, of = iota((256, 192), 0), iota((256, 192), 1)
     place = ((to // 8 == of // SLOTS) & (to % 8 == of % SLOTS)).astype(BF16)
     for b, w_ref in enumerate((w0_ref, w1_ref, w2_ref, w3_ref)):
-        total = jnp.zeros((192, 128), F32)
-        for r in range(4):
-            total = total + jnp.dot(
-                rows_ref[:, r * 512 : (r + 1) * 512],
-                w_ref[0, chunk(held_by(r), 512), :],
-                preferred_element_type=F32,
-            )
+        total = jnp.dot(rows_ref[...], w_ref[0], preferred_element_type=F32)
         placed = jnp.dot(place, total.astype(BF16), preferred_element_type=F32)
         out_ref[:, held_by(b)] = placed.astype(BF16).reshape(32, 8, 128)
 
@@ -182,7 +247,7 @@
         down_kernel,
         name="down",
         compiler_params=LIMIT,
-        out_shape=pltpu.VMEM((32, 4, 8, 128), BF16),
+        out_shape=pltpu.HBM((32, 4, 8, 128), BF16),
         in_specs=vmem(5),
         out_specs=vmem(1)[0],
         scratch_shapes=[pltpu.VMEM((192, 2048), BF16)],
@@ -214,7 +279,7 @@
     )(*near(own, n1, n2, n3), mix_out, shared_down)
 
 
-def combine_kernel(ids_ref, weights_ref, back_ref, shared_ref, mixed_ref, combined_ref, out_ref):
+def gates_kernel(ids_ref, weights_ref, out_ref):
     ids = ids_ref[...]
     code, experts = ordinals(ids)
     weight = jnp.zeros(experts.shape, F32)
@@ -224,17 +289,30 @@
     row = iota(spread.shape, 0)
     wanted = row % 32 // 8 * SLOTS + row % 8 + 1
     here = (spread == wanted.astype(F32)) & (row % 8 < SLOTS)
-    back = back_ref[...].reshape(1024, 128)
-    pieces = []
-    for _ in range(3):
+    for place in range(3):
         piece = weight.astype(BF16)
         weight = weight - piece.astype(F32)
         piece = jnp.dot(expert_of, piece, preferred_element_type=F32)
-        pieces.append(jnp.where(here, piece, 0.0).astype(BF16))
+        out_ref[place] = jnp.where(here, piece, 0.0).astype(BF16)
+
+
+def gates_of(ids, weights):
+    return pl.pallas_call(
+        gates_kernel,
+        name="gates",
+        compiler_params=LIMIT,
+        out_shape=pltpu.VMEM((3, 1024, 128), BF16),
+        in_specs=vmem(2),
+        out_specs=vmem(1)[0],
+    )(ids, weights)
+
+
+def combine_kernel(gates_ref, back_ref, shared_ref, mixed_ref, combined_ref, out_ref):
+    back = back_ref[...].reshape(1024, 128)
     routed = jnp.zeros((128, 128), F32)
-    for piece in reversed(pieces):
+    for place in (2, 1, 0):
         routed = routed + lax.dot_general(
-            piece, back, (((0,), (0,)), ((), ())), preferred_element_type=F32
+            gates_ref[place], back, (((0,), (0,)), ((), ())), preferred_element_type=F32
         )
     combined = routed + shared_ref[...]
     combined_ref[...] = combined
@@ -247,15 +325,15 @@
             out_ref[p, place + 1 : place + 2, :] = square
 
 
-def combine(ids, weights, back, shared, mixed):
+def combine(gates, back, shared, mixed):
     return pl.pallas_call(
         combine_kernel,
         name="combine",
         compiler_params=LIMIT,
-        out_shape=[pltpu.VMEM((128, 128), F32), pltpu.VMEM((16, 4, 128), F32)],
-        in_specs=vmem(5),
+        out_shape=[pltpu.VMEM((128, 128), F32), pltpu.HBM((16, 4, 128), F32)],
+        in_specs=vmem(4),
         out_specs=vmem(2),
-    )(ids, weights, *near(back, shared, mixed))
+    )(*near(gates, back, shared, mixed))
 
 
 def finish_kernel(stats_ref, mixed_ref, combined_ref, coef_ref, out_mixer_ref, out_experts_ref):
@@ -309,49 +387,32 @@
     gain_experts,
     bias_experts,
 ):
-    token_rows, column_count = outer_gate.shape
     ep_count = lax.axis_size("ep")
-    taps_count = conv_taps.shape[0]
     ids = route_ids.T
-    sent, own = pack(
-        ids, moe_input, expert_gate.reshape(2, 1024, 128), expert_up.reshape(2, 1024, 128)
-    )
+    gate_own, up_own = expert_gate.reshape(2048, 128), expert_up.reshape(2048, 128)
+    sent, own = pack(ids, moe_input, gate_own, up_own)
     arrived = exchanged(sent.reshape(ep_count, 24, 128), "ep").reshape(768, 128)
     before, after = rotated(own, 1), rotated(own, -1)
-    far_gate = before[0:2]
-    far_up = after[2:4]
-    gate3, up3 = rotated(far_gate, 1), rotated(far_up, -1)
+    far_low = half_of(before, 0)
+    far_high = half_of(after, 1)
+    low, high = rotated(far_low, 1), rotated(far_high, -1)
     down1, down2 = rotated(expert_down, 1), rotated(expert_down, -1)
     down3 = rotated(expert_down, 2)
 
-    product = (inner_gate.astype(F32) * conv_value.astype(F32)).astype(BF16)
-    border = shifted(product[token_rows - (taps_count - 1) :], "ep", 1)
-    extended = jnp.concatenate([border, product], axis=0).astype(F32)
-    seq_length = token_rows * ep_count // SEQS
-    places = (
-        lax.axis_index("ep") * token_rows + jnp.arange(token_rows, dtype=jnp.int32)
-    ) % seq_length
-    convolved = jnp.zeros((token_rows, column_count), F32)
-    for offset in range(taps_count):
-        delay_rows = taps_count - 1 - offset
-        delayed = extended[offset : offset + token_rows]
-        kept_mask = (places >= delay_rows).astype(F32)[:, None]
-        convolved = convolved + conv_taps[offset].astype(F32)[None, :] * delayed * kept_mask
-    weighted_in = (outer_gate.astype(F32) * convolved).astype(BF16)
-    shared_gate_value = jnp.dot(moe_input, shared_gate, preferred_element_type=F32)
-    shared_up_value = jnp.dot(moe_input, shared_up, preferred_element_type=F32)
-    shared_hidden = (jax.nn.silu(shared_gate_value) * shared_up_value).astype(BF16)
-    both = jnp.concatenate([weighted_in, shared_hidden])
-    rows = exchanged(copies(arrived, both), "x")
-    wide = rows[:, 768:]
+    product, tail, shared_hidden = front(
+        inner_gate, conv_value, moe_input, shared_gate, shared_up
+    )
+    border = shifted(tail, "ep", 1)
+    rows = copies(arrived, border, product, outer_gate, conv_taps, shared_hidden)
+    rows = exchanged(rows, "x")
+    hidden, wide = hidden_of(rows, own, before, after, low, high)
+    hidden = exchanged(hidden, "x")
     mixed, shared_sum = wide_products(
         wide, rotated(wide, 1), rotated(wide, -1), rotated(wide, 2), mix_out, shared_down
     )
-    hidden = hidden_of(rows, expert_gate, expert_up, before, after, gate3, up3)
-    hidden = exchanged(hidden, "x")
     expert_out = down_of(hidden, expert_down, down1, down2, down3)
     back = exchanged(expert_out.reshape(ep_count * 4, 8, 128), ("ep", "y"))
-    combined, stats = combine(ids, route_weights.T, back, shared_sum, mixed)
+    combined, stats = combine(gates_of(ids, route_weights.T), back, shared_sum, mixed)
     stats = exchanged(stats, TP)
     coef = jnp.stack([gain_mixer, bias_mixer, gain_experts, bias_experts]).astype(F32)
     return tuple(finish(stats, mixed, combined, coef))

time: 166 us -> 159 us (0.958)
  local copies, waits for them, and re-layouts: 11.4 us -> 2.42 us
  Pallas kernels: 13.3 us -> 15.3 us
    unnamed x44 -> x32, local copies, waits for them, and re-layouts: 8.69 us -> 2.42 us
    slice x4 -> x0, local copies, waits for them, and re-layouts: 2.75 us -> none  [the longest x1 1.89 us: on_device(): far_up = after[2:4]]
    pallas_call x0 -> x4, Pallas kernels: none -> 2.71 us  [the longest x2 1.67 us: half_of(): pl.pallas_call(half_kernel, name='half', compiler_params=LIMIT, grid=(1,)...]
    ppermute x10, waiting for transfers between devices: 30.1 us -> 28 us  [rotated(): lax.ppermute(x, 'y', [(i, (i + distance) % count) for i in range(count)])]
    all_to_all x5, waiting for transfers between devices: 25.3 us -> 27.2 us  [exchanged(): return lax.all_to_all(x, axis, split_axis=0, concat_axis=0, tiled=True)]
  transfers between devices with their start and end apart: 16 -> 16, of which waited for: 12 -> 11; matrix products, arithmetic and copies ran while one was open for 2% -> 0% of each run, Pallas kernels for 1% -> 3%
where the time goes in v1:
time: 159 us; the launch traced here: 158 us
  starting transfers between devices  83.3 us (52%)
  waiting for transfers between devices  55.9 us (35%)
  Pallas kernels  15.3 us (10%)
  local copies, waits for them, and re-layouts  2.42 us (2%)
    all_to_all x5, starting transfers between devices, exchanged(): return lax.all_to_all(x, axis, split_axis=0, concat_axis=0, tiled=True)  44.2 us
    ppermute x10, starting transfers between devices, rotated(): lax.ppermute(x, 'y', [(i, (i + distance) % count) for i in range(count)])  35.6 us
    ppermute x10, waiting for transfers between devices, rotated(): lax.ppermute(x, 'y', [(i, (i + distance) % count) for i in range(count)])  28 us
    all_to_all x5, waiting for transfers between devices, exchanged(): return lax.all_to_all(x, axis, split_axis=0, concat_axis=0, tiled=True)  27.2 us
    ppermute x1, starting transfers between devices, shifted(): return lax.ppermute(block, axis, route)  3.54 us
    pallas_call x1, Pallas kernels, hidden_of(): pl.pallas_call(hidden_kernel, name='hidden', compiler_params=LIMIT, out_s...  3.49 us
  transfers between devices with their start and end apart: 16, of which 11 were waited for; matrix products, arithmetic and copies ran while one was open for 0% of the time, Pallas kernels for 3%

profile of v1, /device:TPU:1, one launch (start us, length us, event | category | flops | bytes accessed | tf_op | source)
XLA Modules:
  0.0 157.8 jit_solution(6648307537601391412)
XLA Ops:
  0.7 3.0 %pack.1 = (bf16[768,128]{1,0:T(8,128)(2,1)}, bf16[2048,256]{1,0:T(8,128)(2,1)}) custom-call(s32[4,128]{1,0:T(4,128)} %bitcast.12, bf16[128,2048]{1,0:T(8,128)(2,1)} %x_ref.1, bf16[2048,128]{1,0:T(8,128)(2,1)} %bitcast.16, bf16[2048,128]{1,0:T(8,128)(2,1)} %bitcast.17), custom_call_target="tpu_custom_call" | custom-call | tf_op jit(solution)/shard_map/pack/pallas_call | solution.py:113
  3.7 4.0 %collective-permute-start.1 = (bf16[2048,256]{1,0:T(8,128)(2,1)}, bf16[2048,256]{1,0:T(8,128)(2,1)S(1)}, u32[]{:S(2)}, u32[]{:S(2)}) collective-permute-start(bf16[2048,256]{1,0:T(8,128)(2,1)} %get-tuple-element.17.own_ref), channel_id=1, source_target_pairs={{0,4},{4,8},{8,12},{12,0},{1,5},{5,9},{9,13},{13,1},{2,6},{6,10},{... | collective-permute-start | bytes 3145736 | tf_op jit(solution)/shard_map/ppermute | solution.py:24
  7.7 3.4 %collective-permute-start.2 = (bf16[2048,256]{1,0:T(8,128)(2,1)}, bf16[2048,256]{1,0:T(8,128)(2,1)S(1)}, u32[]{:S(2)}, u32[]{:S(2)}) collective-permute-start(bf16[2048,256]{1,0:T(8,128)(2,1)} %get-tuple-element.17.own_ref), channel_id=1, source_target_pairs={{0,12},{4,0},{8,4},{12,8},{1,13},{5,1},{9,5},{13,9},{2,14},{6,2},{... | collective-permute-start | bytes 3145736 | tf_op jit(solution)/shard_map/ppermute | solution.py:24
  11.1 16.4 %all-to-all-start = ((bf16[32,24,128]{2,1,0:T(8,128)(2,1)}), bf16[32,24,128]{2,1,0:T(8,128)(2,1)S(1)}, u32[]{:S(2)}, u32[]{:S(2)}) async-start(bf16[32,24,128]{2,1,0:T(8,128)(2,1)} %bitcast.18), calls=%async_computation | async-start | bytes 393216 | tf_op jit(solution)/shard_map/all_to_all | solution.py:28
  29.1 3.5 %collective-permute-start = (bf16[2,128]{1,0:T(2,128)(2,1)S(1)}, bf16[2,128]{1,0:T(2,128)(2,1)S(1)}, u32[]{:S(2)}, u32[]{:S(2)}) collective-permute-start(bf16[2,128]{1,0:T(2,128)(2,1)S(1)} %get-tuple-element.14), channel_id=1, source_target_pairs={{0,16},{16,32},{32,48},{48,64},{64,80},{80,96},{96,112},{112,128},... | collective-permute-start | bytes 1544 | tf_op jit(solution)/shard_map/ppermute | solution.py:19
  33.3 13.0 %all-to-all-done = bf16[32,24,128]{2,1,0:T(8,128)(2,1)S(1)} async-done(((bf16[32,24,128]{2,1,0:T(8,128)(2,1)}), bf16[32,24,128]{2,1,0:T(8,128)(2,1)S(1)}, u32[]{:S(2)}, u32[]{:S(2)}) %all-to-all-start) | async-done | bytes 196640 | tf_op jit(solution)/shard_map/all_to_all | solution.py:28
  48.1 4.0 %all-to-all-start.1 = ((bf16[4,1024,128]{2,1,0:T(8,128)(2,1)}), bf16[4,1024,128]{2,1,0:T(8,128)(2,1)S(1)}, u32[]{:S(2)}, u32[]{:S(2)}) async-start(bf16[4,1024,128]{2,1,0:T(8,128)(2,1)} %copies.1), calls=%async_computation.1 | async-start | bytes 2097152 | tf_op jit(solution)/shard_map/all_to_all | solution.py:28
  55.8 4.5 %collective-permute-start.4 = (bf16[1024,256]{1,0:T(8,128)(2,1)}, bf16[1024,256]{1,0:T(8,128)(2,1)}, u32[]{:S(2)}, u32[]{:S(2)}) collective-permute-start(bf16[1024,256]{1,0:T(8,128)(2,1)} %half.3), channel_id=1, source_target_pairs={{0,12},{4,0},{8,4},{12,8},{1,13},{5,1},{9,5},{13,9},{2,14},{6,2},{... | collective-permute-start | bytes 1572872 | tf_op jit(solution)/shard_map/ppermute | solution.py:24
  60.3 5.3 %all-to-all-done.1.x_ref = bf16[4,1024,128]{2,1,0:T(8,128)(2,1)S(1)} async-done(((bf16[4,1024,128]{2,1,0:T(8,128)(2,1)}), bf16[4,1024,128]{2,1,0:T(8,128)(2,1)S(1)}, u32[]{:S(2)}, u32[]{:S(2)}) %all-to-all-start.1) | async-done | bytes 1048608 | tf_op jit(solution)/shard_map/all_to_all | solution.py:28
  69.8 3.5 %hidden.1 = (bf16[4,192,512]{2,1,0:T(8,128)(2,1)}, bf16[4,256,128]{2,1,0:T(8,128)(2,1)S(1)}) custom-call(bf16[4,1024,128]{2,1,0:T(8,128)(2,1)S(1)} %all-to-all-done.1.x_ref, bf16[2048,256]{1,0:T(8,128)(2,1)} %get-tuple-element.17.own_ref, bf16[2048,256]{1,0:T(8,128)(2,1)S(1)} %collective-permute-done.1.x_ref.w1_ref, ...), custom_call_target="tpu_custom_call" | custom-call | tf_op jit(solution)/shard_map/hidden/pallas_call | solution.py:218
  73.3 4.1 %all-to-all-start.2 = ((bf16[4,192,512]{2,1,0:T(8,128)(2,1)}), bf16[4,192,512]{2,1,0:T(8,128)(2,1)S(1)}, u32[]{:S(2)}, u32[]{:S(2)}) async-start(bf16[4,192,512]{2,1,0:T(8,128)(2,1)} %get-tuple-element.18), calls=%async_computation.2 | async-start | bytes 1572864 | tf_op jit(solution)/shard_map/all_to_all | solution.py:28
  77.4 2.8 %collective-permute-start.5 = (bf16[1,2048,128]{2,1,0:T(8,128)(2,1)S(1)}, bf16[1,2048,128]{2,1,0:T(8,128)(2,1)S(1)}, u32[]{:S(2)}, u32[]{:S(2)}) collective-permute-start(bf16[1,2048,128]{2,1,0:T(8,128)(2,1)S(1)} %copy-done.3), channel_id=1, source_target_pairs={{0,4},{4,8},{8,12},{12,0},{1,5},{5,9},{9,13},{13,1},{2,6},{6,10},{... | collective-permute-start | bytes 1572872 | tf_op jit(solution)/shard_map/ppermute | solution.py:24
  80.2 4.4 %collective-permute-start.6 = (bf16[1,2048,128]{2,1,0:T(8,128)(2,1)S(1)}, bf16[1,2048,128]{2,1,0:T(8,128)(2,1)S(1)}, u32[]{:S(2)}, u32[]{:S(2)}) collective-permute-start(bf16[1,2048,128]{2,1,0:T(8,128)(2,1)S(1)} %copy-done.3), channel_id=1, source_target_pairs={{0,12},{4,0},{8,4},{12,8},{1,13},{5,1},{9,5},{13,9},{2,14},{6,2},{... | collective-permute-start | bytes 1572872 | tf_op jit(solution)/shard_map/ppermute | solution.py:24
  84.7 3.1 %collective-permute-start.7 = (bf16[1,2048,128]{2,1,0:T(8,128)(2,1)S(1)}, bf16[1,2048,128]{2,1,0:T(8,128)(2,1)S(1)}, u32[]{:S(2)}, u32[]{:S(2)}) collective-permute-start(bf16[1,2048,128]{2,1,0:T(8,128)(2,1)S(1)} %copy-done.3), channel_id=1, source_target_pairs={{0,8},{4,12},{8,0},{12,4},{1,9},{5,13},{9,1},{13,5},{2,10},{6,14},... | collective-permute-start | bytes 1572872 | tf_op jit(solution)/shard_map/ppermute | solution.py:24
  87.8 3.8 %collective-permute-done.5.w1_ref = bf16[1,2048,128]{2,1,0:T(8,128)(2,1)S(1)} collective-permute-done((bf16[1,2048,128]{2,1,0:T(8,128)(2,1)S(1)}, bf16[1,2048,128]{2,1,0:T(8,128)(2,1)S(1)}, u32[]{:S(2)}, u32[]{:S(2)}) %collective-permute-start.5) | collective-permute-done | bytes 524320 | tf_op jit(solution)/shard_map/ppermute | solution.py:24
  93.6 10.1 %collective-permute-done.7.w3_ref = bf16[1,2048,128]{2,1,0:T(8,128)(2,1)S(1)} collective-permute-done((bf16[1,2048,128]{2,1,0:T(8,128)(2,1)S(1)}, bf16[1,2048,128]{2,1,0:T(8,128)(2,1)S(1)}, u32[]{:S(2)}, u32[]{:S(2)}) %collective-permute-start.7) | collective-permute-done | bytes 524320 | tf_op jit(solution)/shard_map/ppermute | solution.py:24
  103.7 2.6 %down.1 = bf16[32,4,8,128]{3,2,1,0:T(8,128)(2,1)} custom-call(bf16[4,192,512]{2,1,0:T(8,128)(2,1)S(1)} %all-to-all-done.2.h_ref, bf16[1,2048,128]{2,1,0:T(8,128)(2,1)S(1)} %copy-done.3, bf16[1,2048,128]{2,1,0:T(8,128)(2,1)S(1)} %collective-permute-done.5.w1_ref, bf16[1,2048,128]{2,1,0:T(8,128)(2,1)S(1)} %collective-permute-done.6.w2_ref, ...), custom_call_target="tpu_custom_call" | custom-call | tf_op jit(solution)/shard_map/down/pallas_call | solution.py:246
  106.3 14.0 %all-to-all-start.3 = ((bf16[128,8,128]{2,1,0:T(8,128)(2,1)}), bf16[128,8,128]{2,1,0:T(8,128)(2,1)S(1)}, u32[]{:S(2)}, u32[]{:S(2)}) async-start(bf16[128,8,128]{2,1,0:T(8,128)(2,1)} %bitcast.15), calls=%async_computation.3 | async-start | bytes 524288 | tf_op jit(solution)/shard_map/all_to_all | solution.py:28
  120.4 4.9 %collective-permute-start.10 = (bf16[4,256,128]{2,1,0:T(8,128)(2,1)S(1)}, bf16[4,256,128]{2,1,0:T(8,128)(2,1)S(1)}, u32[]{:S(2)}, u32[]{:S(2)}) collective-permute-start(bf16[4,256,128]{2,1,0:T(8,128)(2,1)S(1)} %get-tuple-element.19.own_ref), channel_id=1, source_target_pairs={{0,8},{4,12},{8,0},{12,4},{1,9},{5,13},{9,1},{13,5},{2,10},{6,14},... | collective-permute-start | bytes 786440 | tf_op jit(solution)/shard_map/ppermute | solution.py:24
  127.5 4.3 %collective-permute-start.9 = (bf16[4,256,128]{2,1,0:T(8,128)(2,1)S(1)}, bf16[4,256,128]{2,1,0:T(8,128)(2,1)S(1)}, u32[]{:S(2)}, u32[]{:S(2)}) collective-permute-start(bf16[4,256,128]{2,1,0:T(8,128)(2,1)S(1)} %get-tuple-element.19.own_ref), channel_id=1, source_target_pairs={{0,12},{4,0},{8,4},{12,8},{1,13},{5,1},{9,5},{13,9},{2,14},{6,2},{... | collective-permute-start | bytes 786440 | tf_op jit(solution)/shard_map/ppermute | solution.py:24
  132.4 7.7 %collective-permute-done.8.n1_ref = bf16[4,256,128]{2,1,0:T(8,128)(2,1)S(1)} collective-permute-done((bf16[4,256,128]{2,1,0:T(8,128)(2,1)S(1)}, bf16[4,256,128]{2,1,0:T(8,128)(2,1)S(1)}, u32[]{:S(2)}, u32[]{:S(2)}) %collective-permute-start.8) | collective-permute-done | bytes 262176 | tf_op jit(solution)/shard_map/ppermute | solution.py:24
  140.6 3.2 %all-to-all-done.3.back_ref = bf16[128,8,128]{2,1,0:T(8,128)(2,1)S(1)} async-done(((bf16[128,8,128]{2,1,0:T(8,128)(2,1)}), bf16[128,8,128]{2,1,0:T(8,128)(2,1)S(1)}, u32[]{:S(2)}, u32[]{:S(2)}) %all-to-all-start.3) | async-done | bytes 262176 | tf_op jit(solution)/shard_map/all_to_all | solution.py:28
  144.9 5.7 %all-to-all-start.4 = ((f32[16,4,128]{2,1,0:T(4,128)}), f32[16,4,128]{2,1,0:T(4,128)S(1)}, u32[]{:S(2)}, u32[]{:S(2)}) async-start(f32[16,4,128]{2,1,0:T(4,128)} %get-tuple-element.22), calls=%async_computation.4 | async-start | bytes 65536 | tf_op jit(solution)/shard_map/all_to_all | solution.py:28
  151.3 5.7 %all-to-all-done.4.stats_ref = f32[16,4,128]{2,1,0:T(4,128)S(1)} async-done(((f32[16,4,128]{2,1,0:T(4,128)}), f32[16,4,128]{2,1,0:T(4,128)S(1)}, u32[]{:S(2)}, u32[]{:S(2)}) %all-to-all-start.4) | async-done | bytes 32800 | tf_op jit(solution)/shard_map/all_to_all | solution.py:28
  (52 shorter events, 19.7 us)
Async XLA Ops:
  0.6 26.9 %copy-start = (bf16[128,2048]{1,0:T(8,128)(2,1)S(1)}, bf16[128,2048]{1,0:T(8,128)(2,1)}, u32[]{:S(2)}) copy-start(bf16[128,2048]{1,0:T(8,128)(2,1)} %x_ref.1) | copy-start | bytes 1572868
  0.6 26.9 %copy-start.1 = (bf16[2048,128]{1,0:T(8,128)(2,1)S(1)}, bf16[2048,128]{1,0:T(8,128)(2,1)}, u32[]{:S(2)}) copy-start(bf16[2048,128]{1,0:T(8,128)(2,1)} %gate_ref.1) | copy-start | bytes 1572868
  3.7 48.4 %collective-permute-start.1 = (bf16[2048,256]{1,0:T(8,128)(2,1)}, bf16[2048,256]{1,0:T(8,128)(2,1)S(1)}, u32[]{:S(2)}, u32[]{:S(2)}) collective-permute-start(bf16[2048,256]{1,0:T(8,128)(2,1)} %get-tuple-element.17.own_ref), channel_id=1, source_target_pairs={{0,4},{4,8},{8,12},{12,0},{1,5},{5,9},{9,13},{13,1},{2,6},{6,10},{... | collective-permute-start | bytes 3145736 | tf_op jit(solution)/shard_map/ppermute | solution.py:24
  7.7 47.2 %collective-permute-start.2 = (bf16[2048,256]{1,0:T(8,128)(2,1)}, bf16[2048,256]{1,0:T(8,128)(2,1)S(1)}, u32[]{:S(2)}, u32[]{:S(2)}) collective-permute-start(bf16[2048,256]{1,0:T(8,128)(2,1)} %get-tuple-element.17.own_ref), channel_id=1, source_target_pairs={{0,12},{4,0},{8,4},{12,8},{1,13},{5,1},{9,5},{13,9},{2,14},{6,2},{... | collective-permute-start | bytes 3145736 | tf_op jit(solution)/shard_map/ppermute | solution.py:24
  11.1 16.5 %copy-start.6 = (bf16[128,128]{1,0:T(8,128)(2,1)S(1)}, bf16[128,128]{1,0:T(8,128)(2,1)}, u32[]{:S(2)}) copy-start(bf16[128,128]{1,0:T(8,128)(2,1)} %inner_ref.1) | copy-start | bytes 98308
  11.1 35.2 %all-to-all-start = ((bf16[32,24,128]{2,1,0:T(8,128)(2,1)}), bf16[32,24,128]{2,1,0:T(8,128)(2,1)S(1)}, u32[]{:S(2)}, u32[]{:S(2)}) async-start(bf16[32,24,128]{2,1,0:T(8,128)(2,1)} %bitcast.18), calls=%async_computation | async-start | bytes 393216 | tf_op jit(solution)/shard_map/all_to_all | solution.py:28
  28.6 17.7 %copy-start.8 = (bf16[128,128]{1,0:T(8,128)(2,1)S(1)}, bf16[128,128]{1,0:T(8,128)(2,1)}, u32[]{:S(2)}) copy-start(bf16[128,128]{1,0:T(8,128)(2,1)} %outer_ref.1) | copy-start | bytes 98308
  29.1 4.2 %collective-permute-start = (bf16[2,128]{1,0:T(2,128)(2,1)S(1)}, bf16[2,128]{1,0:T(2,128)(2,1)S(1)}, u32[]{:S(2)}, u32[]{:S(2)}) collective-permute-start(bf16[2,128]{1,0:T(2,128)(2,1)S(1)} %get-tuple-element.14), channel_id=1, source_target_pairs={{0,16},{16,32},{32,48},{48,64},{64,80},{80,96},{96,112},{112,128},... | collective-permute-start | bytes 1544 | tf_op jit(solution)/shard_map/ppermute | solution.py:19
  48.1 17.5 %all-to-all-start.1 = ((bf16[4,1024,128]{2,1,0:T(8,128)(2,1)}), bf16[4,1024,128]{2,1,0:T(8,128)(2,1)S(1)}, u32[]{:S(2)}, u32[]{:S(2)}) async-start(bf16[4,1024,128]{2,1,0:T(8,128)(2,1)} %copies.1), calls=%async_computation.1 | async-start | bytes 2097152 | tf_op jit(solution)/shard_map/all_to_all | solution.py:28
  52.9 15.2 %collective-permute-start.3 = (bf16[1024,256]{1,0:T(8,128)(2,1)}, bf16[1024,256]{1,0:T(8,128)(2,1)}, u32[]{:S(2)}, u32[]{:S(2)}) collective-permute-start(bf16[1024,256]{1,0:T(8,128)(2,1)} %half.2), channel_id=1, source_target_pairs={{0,4},{4,8},{8,12},{12,0},{1,5},{5,9},{9,13},{13,1},{2,6},{6,10},{... | collective-permute-start | bytes 1572872 | tf_op jit(solution)/shard_map/ppermute | solution.py:24
  55.8 14.1 %collective-permute-start.4 = (bf16[1024,256]{1,0:T(8,128)(2,1)}, bf16[1024,256]{1,0:T(8,128)(2,1)}, u32[]{:S(2)}, u32[]{:S(2)}) collective-permute-start(bf16[1024,256]{1,0:T(8,128)(2,1)} %half.3), channel_id=1, source_target_pairs={{0,12},{4,0},{8,4},{12,8},{1,13},{5,1},{9,5},{13,9},{2,14},{6,2},{... | collective-permute-start | bytes 1572872 | tf_op jit(solution)/shard_map/ppermute | solution.py:24
  73.3 30.4 %all-to-all-start.2 = ((bf16[4,192,512]{2,1,0:T(8,128)(2,1)}), bf16[4,192,512]{2,1,0:T(8,128)(2,1)S(1)}, u32[]{:S(2)}, u32[]{:S(2)}) async-start(bf16[4,192,512]{2,1,0:T(8,128)(2,1)} %get-tuple-element.18), calls=%async_computation.2 | async-start | bytes 1572864 | tf_op jit(solution)/shard_map/all_to_all | solution.py:28
  77.4 14.2 %collective-permute-start.5 = (bf16[1,2048,128]{2,1,0:T(8,128)(2,1)S(1)}, bf16[1,2048,128]{2,1,0:T(8,128)(2,1)S(1)}, u32[]{:S(2)}, u32[]{:S(2)}) collective-permute-start(bf16[1,2048,128]{2,1,0:T(8,128)(2,1)S(1)} %copy-done.3), channel_id=1, source_target_pairs={{0,4},{4,8},{8,12},{12,0},{1,5},{5,9},{9,13},{13,1},{2,6},{6,10},{... | collective-permute-start | bytes 1572872 | tf_op jit(solution)/shard_map/ppermute | solution.py:24
  80.2 13.4 %collective-permute-start.6 = (bf16[1,2048,128]{2,1,0:T(8,128)(2,1)S(1)}, bf16[1,2048,128]{2,1,0:T(8,128)(2,1)S(1)}, u32[]{:S(2)}, u32[]{:S(2)}) collective-permute-start(bf16[1,2048,128]{2,1,0:T(8,128)(2,1)S(1)} %copy-done.3), channel_id=1, source_target_pairs={{0,12},{4,0},{8,4},{12,8},{1,13},{5,1},{9,5},{13,9},{2,14},{6,2},{... | collective-permute-start | bytes 1572872 | tf_op jit(solution)/shard_map/ppermute | solution.py:24
  84.7 19.1 %collective-permute-start.7 = (bf16[1,2048,128]{2,1,0:T(8,128)(2,1)S(1)}, bf16[1,2048,128]{2,1,0:T(8,128)(2,1)S(1)}, u32[]{:S(2)}, u32[]{:S(2)}) collective-permute-start(bf16[1,2048,128]{2,1,0:T(8,128)(2,1)S(1)} %copy-done.3), channel_id=1, source_target_pairs={{0,8},{4,12},{8,0},{12,4},{1,9},{5,13},{9,1},{13,5},{2,10},{6,14},... | collective-permute-start | bytes 1572872 | tf_op jit(solution)/shard_map/ppermute | solution.py:24
  106.3 25.4 %copy-start.10 = (f32[128,4]{0,1:T(4,128)S(1)}, f32[128,4]{0,1:T(4,128)}, u32[]{:S(2)}) copy-start(f32[128,4]{0,1:T(4,128)} %param.27) | copy-start | bytes 6148
  106.3 25.5 %copy-start.9 = (s32[128,4]{0,1:T(4,128)S(1)}, s32[128,4]{0,1:T(4,128)}, u32[]{:S(2)}) copy-start(s32[128,4]{0,1:T(4,128)} %param.26) | copy-start | bytes 6148
  106.3 33.8 %copy-start.5 = (bf16[2048,128]{1,0:T(8,128)(2,1)S(1)}, bf16[2048,128]{1,0:T(8,128)(2,1)}, u32[]{:S(2)}) copy-start(bf16[2048,128]{1,0:T(8,128)(2,1)} %shared_ref.1) | copy-start | bytes 1572868
  106.3 37.4 %all-to-all-start.3 = ((bf16[128,8,128]{2,1,0:T(8,128)(2,1)}), bf16[128,8,128]{2,1,0:T(8,128)(2,1)S(1)}, u32[]{:S(2)}, u32[]{:S(2)}) async-start(bf16[128,8,128]{2,1,0:T(8,128)(2,1)} %bitcast.15), calls=%async_computation.3 | async-start | bytes 524288 | tf_op jit(solution)/shard_map/all_to_all | solution.py:28
  120.4 19.8 %copy-start.4 = (bf16[2048,128]{1,0:T(8,128)(2,1)S(1)}, bf16[2048,128]{1,0:T(8,128)(2,1)}, u32[]{:S(2)}) copy-start(bf16[2048,128]{1,0:T(8,128)(2,1)} %mix_ref.1) | copy-start | bytes 1572868
  120.4 12.1 %collective-permute-start.10 = (bf16[4,256,128]{2,1,0:T(8,128)(2,1)S(1)}, bf16[4,256,128]{2,1,0:T(8,128)(2,1)S(1)}, u32[]{:S(2)}, u32[]{:S(2)}) collective-permute-start(bf16[4,256,128]{2,1,0:T(8,128)(2,1)S(1)} %get-tuple-element.19.own_ref), channel_id=1, source_target_pairs={{0,8},{4,12},{8,0},{12,4},{1,9},{5,13},{9,1},{13,5},{2,10},{6,14},... | collective-permute-start | bytes 786440 | tf_op jit(solution)/shard_map/ppermute | solution.py:24
  125.3 14.9 %collective-permute-start.8 = (bf16[4,256,128]{2,1,0:T(8,128)(2,1)S(1)}, bf16[4,256,128]{2,1,0:T(8,128)(2,1)S(1)}, u32[]{:S(2)}, u32[]{:S(2)}) collective-permute-start(bf16[4,256,128]{2,1,0:T(8,128)(2,1)S(1)} %get-tuple-element.19.own_ref), channel_id=1, source_target_pairs={{0,4},{4,8},{8,12},{12,0},{1,5},{5,9},{9,13},{13,1},{2,6},{6,10},{... | collective-permute-start | bytes 786440 | tf_op jit(solution)/shard_map/ppermute | solution.py:24
  127.5 12.7 %collective-permute-start.9 = (bf16[4,256,128]{2,1,0:T(8,128)(2,1)S(1)}, bf16[4,256,128]{2,1,0:T(8,128)(2,1)S(1)}, u32[]{:S(2)}, u32[]{:S(2)}) collective-permute-start(bf16[4,256,128]{2,1,0:T(8,128)(2,1)S(1)} %get-tuple-element.19.own_ref), channel_id=1, source_target_pairs={{0,12},{4,0},{8,4},{12,8},{1,13},{5,1},{9,5},{13,9},{2,14},{6,2},{... | collective-permute-start | bytes 786440 | tf_op jit(solution)/shard_map/ppermute | solution.py:24
  144.9 12.2 %all-to-all-start.4 = ((f32[16,4,128]{2,1,0:T(4,128)}), f32[16,4,128]{2,1,0:T(4,128)S(1)}, u32[]{:S(2)}, u32[]{:S(2)}) async-start(f32[16,4,128]{2,1,0:T(4,128)} %get-tuple-element.22), calls=%async_computation.4 | async-start | bytes 65536 | tf_op jit(solution)/shard_map/all_to_all | solution.py:28
  (8 other events, 31.1 us)

commit v2 on v1

--- a/solution.py
+++ b/solution.py
@@ -127,22 +127,6 @@
     )(*far(ids, x, gate, up))
 
 
-def half_kernel(x_ref, out_ref):
-    out_ref[...] = x_ref[...]
-
-
-def half_of(x, place):
-    return pl.pallas_call(
-        half_kernel,
-        name="half",
-        compiler_params=LIMIT,
-        grid=(1,),
-        out_shape=pltpu.VMEM((1024, 256), BF16),
-        in_specs=[pl.BlockSpec((1024, 256), lambda i: (place, 0))],
-        out_specs=pl.BlockSpec((1024, 256), lambda i: (0, 0)),
-    )(x)
-
-
 def front_kernel(inner_ref, value_ref, x_ref, gate_ref, up_ref, product_ref, tail_ref, hidden_ref):
     product = (inner_ref[...].astype(F32) * value_ref[...].astype(F32)).astype(BF16)
     product_ref[...] = product
@@ -192,7 +176,7 @@
     )(*near(arrived, border, product), outer, taps, *near(shared))
 
 
-def hidden_kernel(x_ref, own_ref, w1_ref, w2_ref, low_ref, high_ref, out_ref, rest_ref, wide_ref, rows_ref):
+def hidden_kernel(x_ref, own_ref, w1_ref, w2_ref, w3_ref, out_ref, rest_ref, wide_ref, rows_ref):
     for q in range(4):
         wide_ref[...] = x_ref[q, 0:768, :].astype(F32)
         for b in range(4):
@@ -200,14 +184,8 @@
                 pl.ds(b, 192, stride=4), :
             ].astype(BF16)
         rest_ref[q] = x_ref[q, 768:1024, :]
-    for r in range(4):
-        if r < 3:
-            ref = (own_ref, w1_ref, w2_ref)[r]
-            both = jnp.dot(rows_ref[...], ref[...], preferred_element_type=F32)
-        else:
-            both = jnp.dot(
-                rows_ref[:, 0:1024], low_ref[...], preferred_element_type=F32
-            ) + jnp.dot(rows_ref[:, 1024:2048], high_ref[...], preferred_element_type=F32)
+    for r, ref in enumerate((own_ref, w1_ref, w2_ref, w3_ref)):
+        both = jnp.dot(rows_ref[...], ref[...], preferred_element_type=F32)
         gate, up = both[:, 0:128], both[:, 128:256]
         hidden = (gate / (1.0 + jnp.exp(-gate)) * up).astype(BF16)
         for q in range(4):
@@ -220,7 +198,7 @@
         name="hidden",
         compiler_params=LIMIT,
         out_shape=[pltpu.HBM((4, 192, 512), BF16), pltpu.VMEM((4, 256, 128), BF16)],
-        in_specs=vmem(6),
+        in_specs=vmem(5),
         out_specs=vmem(2),
         scratch_shapes=[pltpu.VMEM((768, 128), F32), pltpu.VMEM((192, 2048), BF16)],
     )(*near(x), *weights)
@@ -393,11 +371,9 @@
     sent, own = pack(ids, moe_input, gate_own, up_own)
     arrived = exchanged(sent.reshape(ep_count, 24, 128), "ep").reshape(768, 128)
     before, after = rotated(own, 1), rotated(own, -1)
-    far_low = half_of(before, 0)
-    far_high = half_of(after, 1)
-    low, high = rotated(far_low, 1), rotated(far_high, -1)
+    beyond = rotated(before, 1)
     down1, down2 = rotated(expert_down, 1), rotated(expert_down, -1)
-    down3 = rotated(expert_down, 2)
+    down3 = rotated(down2, -1)
 
     product, tail, shared_hidden = front(
         inner_gate, conv_value, moe_input, shared_gate, shared_up
@@ -405,7 +381,7 @@
     border = shifted(tail, "ep", 1)
     rows = copies(arrived, border, product, outer_gate, conv_taps, shared_hidden)
     rows = exchanged(rows, "x")
-    hidden, wide = hidden_of(rows, own, before, after, low, high)
+    hidden, wide = hidden_of(rows, own, before, after, beyond)
     hidden = exchanged(hidden, "x")
     mixed, shared_sum = wide_products(
         wide, rotated(wide, 1), rotated(wide, -1), rotated(wide, 2), mix_out, shared_down

time: 159 us -> 149 us (0.937)
  waiting for transfers between devices: 55.9 us -> 38.4 us
  starting transfers between devices: 83.3 us -> 91.3 us
    ppermute x10 -> x9, waiting for transfers between devices: 28 us -> 18.4 us  [rotated(): lax.ppermute(x, 'y', [(i, (i + distance) % count) for i in range(count)])]
    all_to_all x5, waiting for transfers between devices: 27.2 us -> 19.3 us  [exchanged(): return lax.all_to_all(x, axis, split_axis=0, concat_axis=0, tiled=True)]
    all_to_all x5, starting transfers between devices: 44.2 us -> 52 us  [exchanged(): return lax.all_to_all(x, axis, split_axis=0, concat_axis=0, tiled=True)]
    ppermute x1, starting transfers between devices: 3.54 us -> 6.14 us  [shifted(): return lax.ppermute(block, axis, route)]
    ppermute x10 -> x9, starting transfers between devices: 35.6 us -> 33.1 us  [rotated(): lax.ppermute(x, 'y', [(i, (i + distance) % count) for i in range(count)])]
    pallas_call x2 -> x0, Pallas kernels: 1.67 us -> none  [half_of(): pl.pallas_call(half_kernel, name='half', compiler_params=LIMIT, grid=(1,)...]
  transfers between devices with their start and end apart: 16 -> 15, of which waited for: 11 -> 10; matrix products, arithmetic and copies ran while one was open for 0% -> 0% of each run, Pallas kernels for 3% -> 4%
where the time goes in v2:
time: 149 us; the launch traced here: 148 us
  starting transfers between devices  91.3 us (61%)
  waiting for transfers between devices  38.4 us (26%)
  Pallas kernels  14.3 us (10%)
  local copies, waits for them, and re-layouts  3.46 us (2%)
    all_to_all x5, starting transfers between devices, exchanged(): return lax.all_to_all(x, axis, split_axis=0, concat_axis=0, tiled=True)  52 us
    ppermute x9, starting transfers between devices, rotated(): lax.ppermute(x, 'y', [(i, (i + distance) % count) for i in range(count)])  33.1 us
    all_to_all x5, waiting for transfers between devices, exchanged(): return lax.all_to_all(x, axis, split_axis=0, concat_axis=0, tiled=True)  19.3 us
    ppermute x9, waiting for transfers between devices, rotated(): lax.ppermute(x, 'y', [(i, (i + distance) % count) for i in range(count)])  18.4 us
    ppermute x1, starting transfers between devices, shifted(): return lax.ppermute(block, axis, route)  6.14 us
    pallas_call x1, Pallas kernels, down_of(): pl.pallas_call(down_kernel, name='down', compiler_params=LIMIT, out_shape...  3.66 us
    pallas_call x1, Pallas kernels, hidden_of(): pl.pallas_call(hidden_kernel, name='hidden', compiler_params=LIMIT, out_s...  3.54 us
    unnamed x32, local copies, waits for them, and re-layouts  3.46 us
  transfers between devices with their start and end apart: 15, of which 10 were waited for; matrix products, arithmetic and copies ran while one was open for 0% of the time, Pallas kernels for 4%

profile of v2, /device:TPU:1, one launch (start us, length us, event | category | flops | bytes accessed | tf_op | source)
XLA Modules:
  0.0 148.4 jit_solution(11941827966777260360)
XLA Ops:
  0.6 2.6 %pack.1 = (bf16[768,128]{1,0:T(8,128)(2,1)}, bf16[2048,256]{1,0:T(8,128)(2,1)S(1)}) custom-call(s32[4,128]{1,0:T(4,128)} %bitcast.12, bf16[128,2048]{1,0:T(8,128)(2,1)} %x_ref.1, bf16[2048,128]{1,0:T(8,128)(2,1)} %bitcast.16, bf16[2048,128]{1,0:T(8,128)(2,1)} %bitcast.17), custom_call_target="tpu_custom_call" | custom-call | tf_op jit(solution)/shard_map/pack/pallas_call | solution.py:113
  3.3 4.0 %collective-permute-start.1 = (bf16[2048,256]{1,0:T(8,128)(2,1)S(1)}, bf16[2048,256]{1,0:T(8,128)(2,1)S(1)}, u32[]{:S(2)}, u32[]{:S(2)}) collective-permute-start(bf16[2048,256]{1,0:T(8,128)(2,1)S(1)} %get-tuple-element.17.own_ref), channel_id=1, source_target_pairs={{0,4},{4,8},{8,12},{12,0},{1,5},{5,9},{9,13},{13,1},{2,6},{6,10},{... | collective-permute-start | bytes 3145736 | tf_op jit(solution)/shard_map/ppermute | solution.py:24
  7.3 16.3 %all-to-all-start = ((bf16[32,24,128]{2,1,0:T(8,128)(2,1)}), bf16[32,24,128]{2,1,0:T(8,128)(2,1)S(1)}, u32[]{:S(2)}, u32[]{:S(2)}) async-start(bf16[32,24,128]{2,1,0:T(8,128)(2,1)} %bitcast.18), calls=%async_computation | async-start | bytes 393216 | tf_op jit(solution)/shard_map/all_to_all | solution.py:28
  23.7 3.3 %collective-permute-start.2 = (bf16[2048,256]{1,0:T(8,128)(2,1)S(1)}, bf16[2048,256]{1,0:T(8,128)(2,1)}, u32[]{:S(2)}, u32[]{:S(2)}) collective-permute-start(bf16[2048,256]{1,0:T(8,128)(2,1)S(1)} %get-tuple-element.17.own_ref), channel_id=1, source_target_pairs={{0,12},{4,0},{8,4},{12,8},{1,13},{5,1},{9,5},{13,9},{2,14},{6,2},{... | collective-permute-start | bytes 3145736 | tf_op jit(solution)/shard_map/ppermute | solution.py:24
  27.0 5.3 %collective-permute-start.3 = (bf16[2048,256]{1,0:T(8,128)(2,1)S(1)}, bf16[2048,256]{1,0:T(8,128)(2,1)}, u32[]{:S(2)}, u32[]{:S(2)}) collective-permute-start(bf16[2048,256]{1,0:T(8,128)(2,1)S(1)} %collective-permute-done.1.w1_ref), channel_id=1, source_target_pairs={{0,4},{4,8},{8,12},{12,0},{1,5},{5,9},{9,13},{13,1},{2,6},{6,10},{... | collective-permute-start | bytes 3145736 | tf_op jit(solution)/shard_map/ppermute | solution.py:24
  34.9 6.1 %collective-permute-start = (bf16[2,128]{1,0:T(2,128)(2,1)S(1)}, bf16[2,128]{1,0:T(2,128)(2,1)S(1)}, u32[]{:S(2)}, u32[]{:S(2)}) collective-permute-start(bf16[2,128]{1,0:T(2,128)(2,1)S(1)} %get-tuple-element.14), channel_id=1, source_target_pairs={{0,16},{16,32},{32,48},{48,64},{64,80},{80,96},{96,112},{112,128},... | collective-permute-start | bytes 1544 | tf_op jit(solution)/shard_map/ppermute | solution.py:19
  44.3 4.0 %all-to-all-start.1 = ((bf16[4,1024,128]{2,1,0:T(8,128)(2,1)}), bf16[4,1024,128]{2,1,0:T(8,128)(2,1)S(1)}, u32[]{:S(2)}, u32[]{:S(2)}) async-start(bf16[4,1024,128]{2,1,0:T(8,128)(2,1)} %copies.1), calls=%async_computation.1 | async-start | bytes 2097152 | tf_op jit(solution)/shard_map/all_to_all | solution.py:28
  48.3 3.8 %collective-permute-start.5 = (bf16[1,2048,128]{2,1,0:T(8,128)(2,1)}, bf16[1,2048,128]{2,1,0:T(8,128)(2,1)}, u32[]{:S(2)}, u32[]{:S(2)}) collective-permute-start(bf16[1,2048,128]{2,1,0:T(8,128)(2,1)} %w0_ref.1), channel_id=1, source_target_pairs={{0,12},{4,0},{8,4},{12,8},{1,13},{5,1},{9,5},{13,9},{2,14},{6,2},{... | collective-permute-start | bytes 1572872 | tf_op jit(solution)/shard_map/ppermute | solution.py:24
  52.1 9.6 %all-to-all-done.1.x_ref = bf16[4,1024,128]{2,1,0:T(8,128)(2,1)S(1)} async-done(((bf16[4,1024,128]{2,1,0:T(8,128)(2,1)}), bf16[4,1024,128]{2,1,0:T(8,128)(2,1)S(1)}, u32[]{:S(2)}, u32[]{:S(2)}) %all-to-all-start.1) | async-done | bytes 1048608 | tf_op jit(solution)/shard_map/all_to_all | solution.py:28
  61.7 3.5 %hidden.1 = (bf16[4,192,512]{2,1,0:T(8,128)(2,1)}, bf16[4,256,128]{2,1,0:T(8,128)(2,1)S(1)}) custom-call(bf16[4,1024,128]{2,1,0:T(8,128)(2,1)S(1)} %all-to-all-done.1.x_ref, bf16[2048,256]{1,0:T(8,128)(2,1)S(1)} %get-tuple-element.17.own_ref, bf16[2048,256]{1,0:T(8,128)(2,1)S(1)} %collective-permute-done.1.w1_ref, ...), custom_call_target="tpu_custom_call" | custom-call | tf_op jit(solution)/shard_map/hidden/pallas_call | solution.py:196
  65.3 3.6 %all-to-all-start.2 = ((bf16[4,192,512]{2,1,0:T(8,128)(2,1)}), bf16[4,192,512]{2,1,0:T(8,128)(2,1)S(1)}, u32[]{:S(2)}, u32[]{:S(2)}) async-start(bf16[4,192,512]{2,1,0:T(8,128)(2,1)} %get-tuple-element.18), calls=%async_computation.2 | async-start | bytes 1572864 | tf_op jit(solution)/shard_map/all_to_all | solution.py:28
  68.9 3.2 %collective-permute-start.4 = (bf16[1,2048,128]{2,1,0:T(8,128)(2,1)S(1)}, bf16[1,2048,128]{2,1,0:T(8,128)(2,1)S(1)}, u32[]{:S(2)}, u32[]{:S(2)}) collective-permute-start(bf16[1,2048,128]{2,1,0:T(8,128)(2,1)S(1)} %copy-done.3), channel_id=1, source_target_pairs={{0,4},{4,8},{8,12},{12,0},{1,5},{5,9},{9,13},{13,1},{2,6},{6,10},{... | collective-permute-start | bytes 1572872 | tf_op jit(solution)/shard_map/ppermute | solution.py:24
  72.1 3.3 %collective-permute-start.6 = (bf16[1,2048,128]{2,1,0:T(8,128)(2,1)}, bf16[1,2048,128]{2,1,0:T(8,128)(2,1)S(1)}, u32[]{:S(2)}, u32[]{:S(2)}) collective-permute-start(bf16[1,2048,128]{2,1,0:T(8,128)(2,1)} %collective-permute-done.5.w2_ref), channel_id=1, source_target_pairs={{0,12},{4,0},{8,4},{12,8},{1,13},{5,1},{9,5},{13,9},{2,14},{6,2},{... | collective-permute-start | bytes 1572872 | tf_op jit(solution)/shard_map/ppermute | solution.py:24
  75.4 7.5 %collective-permute-done.4.w1_ref = bf16[1,2048,128]{2,1,0:T(8,128)(2,1)S(1)} collective-permute-done((bf16[1,2048,128]{2,1,0:T(8,128)(2,1)S(1)}, bf16[1,2048,128]{2,1,0:T(8,128)(2,1)S(1)}, u32[]{:S(2)}, u32[]{:S(2)}) %collective-permute-start.4) | collective-permute-done | bytes 524320 | tf_op jit(solution)/shard_map/ppermute | solution.py:24
  84.9 3.7 %down.1 = bf16[32,4,8,128]{3,2,1,0:T(8,128)(2,1)} custom-call(bf16[4,192,512]{2,1,0:T(8,128)(2,1)S(1)} %all-to-all-done.2.h_ref, bf16[1,2048,128]{2,1,0:T(8,128)(2,1)S(1)} %copy-done.3, bf16[1,2048,128]{2,1,0:T(8,128)(2,1)S(1)} %collective-permute-done.4.w1_ref, bf16[1,2048,128]{2,1,0:T(8,128)(2,1)} %collective-permute-done.5.w2_ref, ...), custom_call_target="tpu_custom_call" | custom-call | tf_op jit(solution)/shard_map/down/pallas_call | solution.py:224
  88.5 22.4 %all-to-all-start.3 = ((bf16[128,8,128]{2,1,0:T(8,128)(2,1)}), bf16[128,8,128]{2,1,0:T(8,128)(2,1)S(1)}, u32[]{:S(2)}, u32[]{:S(2)}) async-start(bf16[128,8,128]{2,1,0:T(8,128)(2,1)} %bitcast.15), calls=%async_computation.3 | async-start | bytes 524288 | tf_op jit(solution)/shard_map/all_to_all | solution.py:28
  111.0 3.4 %collective-permute-start.7 = (bf16[4,256,128]{2,1,0:T(8,128)(2,1)S(1)}, bf16[4,256,128]{2,1,0:T(8,128)(2,1)S(1)}, u32[]{:S(2)}, u32[]{:S(2)}) collective-permute-start(bf16[4,256,128]{2,1,0:T(8,128)(2,1)S(1)} %get-tuple-element.19.own_ref), channel_id=1, source_target_pairs={{0,4},{4,8},{8,12},{12,0},{1,5},{5,9},{9,13},{13,1},{2,6},{6,10},{... | collective-permute-start | bytes 786440 | tf_op jit(solution)/shard_map/ppermute | solution.py:24
  114.4 3.2 %collective-permute-start.8 = (bf16[4,256,128]{2,1,0:T(8,128)(2,1)S(1)}, bf16[4,256,128]{2,1,0:T(8,128)(2,1)S(1)}, u32[]{:S(2)}, u32[]{:S(2)}) collective-permute-start(bf16[4,256,128]{2,1,0:T(8,128)(2,1)S(1)} %get-tuple-element.19.own_ref), channel_id=1, source_target_pairs={{0,12},{4,0},{8,4},{12,8},{1,13},{5,1},{9,5},{13,9},{2,14},{6,2},{... | collective-permute-start | bytes 786440 | tf_op jit(solution)/shard_map/ppermute | solution.py:24
  117.6 3.6 %collective-permute-start.9 = (bf16[4,256,128]{2,1,0:T(8,128)(2,1)S(1)}, bf16[4,256,128]{2,1,0:T(8,128)(2,1)S(1)}, u32[]{:S(2)}, u32[]{:S(2)}) collective-permute-start(bf16[4,256,128]{2,1,0:T(8,128)(2,1)S(1)} %get-tuple-element.19.own_ref), channel_id=1, source_target_pairs={{0,8},{4,12},{8,0},{12,4},{1,9},{5,13},{9,1},{13,5},{2,10},{6,14},... | collective-permute-start | bytes 786440 | tf_op jit(solution)/shard_map/ppermute | solution.py:24
  122.6 2.4 %collective-permute-done.8.n2_ref = bf16[4,256,128]{2,1,0:T(8,128)(2,1)S(1)} collective-permute-done((bf16[4,256,128]{2,1,0:T(8,128)(2,1)S(1)}, bf16[4,256,128]{2,1,0:T(8,128)(2,1)S(1)}, u32[]{:S(2)}, u32[]{:S(2)}) %collective-permute-start.8) | collective-permute-done | bytes 262176 | tf_op jit(solution)/shard_map/ppermute | solution.py:24
  125.0 5.8 %collective-permute-done.9.n3_ref = bf16[4,256,128]{2,1,0:T(8,128)(2,1)S(1)} collective-permute-done((bf16[4,256,128]{2,1,0:T(8,128)(2,1)S(1)}, bf16[4,256,128]{2,1,0:T(8,128)(2,1)S(1)}, u32[]{:S(2)}, u32[]{:S(2)}) %collective-permute-start.9) | collective-permute-done | bytes 262176 | tf_op jit(solution)/shard_map/ppermute | solution.py:24
  131.2 3.2 %all-to-all-done.3.back_ref = bf16[128,8,128]{2,1,0:T(8,128)(2,1)S(1)} async-done(((bf16[128,8,128]{2,1,0:T(8,128)(2,1)}), bf16[128,8,128]{2,1,0:T(8,128)(2,1)S(1)}, u32[]{:S(2)}, u32[]{:S(2)}) %all-to-all-start.3) | async-done | bytes 262176 | tf_op jit(solution)/shard_map/all_to_all | solution.py:28
  135.5 5.6 %all-to-all-start.4 = ((f32[16,4,128]{2,1,0:T(4,128)}), f32[16,4,128]{2,1,0:T(4,128)S(1)}, u32[]{:S(2)}, u32[]{:S(2)}) async-start(f32[16,4,128]{2,1,0:T(4,128)} %get-tuple-element.22), calls=%async_computation.4 | async-start | bytes 65536 | tf_op jit(solution)/shard_map/all_to_all | solution.py:28
  141.8 5.7 %all-to-all-done.4.stats_ref = f32[16,4,128]{2,1,0:T(4,128)S(1)} async-done(((f32[16,4,128]{2,1,0:T(4,128)}), f32[16,4,128]{2,1,0:T(4,128)S(1)}, u32[]{:S(2)}, u32[]{:S(2)}) %all-to-all-start.4) | async-done | bytes 32800 | tf_op jit(solution)/shard_map/all_to_all | solution.py:28
  (48 shorter events, 12.1 us)
Async XLA Ops:
  0.6 31.7 %copy-start = (bf16[128,2048]{1,0:T(8,128)(2,1)S(1)}, bf16[128,2048]{1,0:T(8,128)(2,1)}, u32[]{:S(2)}) copy-start(bf16[128,2048]{1,0:T(8,128)(2,1)} %x_ref.1) | copy-start | bytes 1572868
  3.3 23.7 %collective-permute-start.1 = (bf16[2048,256]{1,0:T(8,128)(2,1)S(1)}, bf16[2048,256]{1,0:T(8,128)(2,1)S(1)}, u32[]{:S(2)}, u32[]{:S(2)}) collective-permute-start(bf16[2048,256]{1,0:T(8,128)(2,1)S(1)} %get-tuple-element.17.own_ref), channel_id=1, source_target_pairs={{0,4},{4,8},{8,12},{12,0},{1,5},{5,9},{9,13},{13,1},{2,6},{6,10},{... | collective-permute-start | bytes 3145736 | tf_op jit(solution)/shard_map/ppermute | solution.py:24
  7.3 25.0 %copy-start.6 = (bf16[128,128]{1,0:T(8,128)(2,1)S(1)}, bf16[128,128]{1,0:T(8,128)(2,1)}, u32[]{:S(2)}) copy-start(bf16[128,128]{1,0:T(8,128)(2,1)} %inner_ref.1) | copy-start | bytes 98308
  7.3 25.0 %copy-start.7 = (bf16[128,128]{1,0:T(8,128)(2,1)S(1)}, bf16[128,128]{1,0:T(8,128)(2,1)}, u32[]{:S(2)}) copy-start(bf16[128,128]{1,0:T(8,128)(2,1)} %value_ref.1) | copy-start | bytes 98308
  7.3 35.2 %copy-start.8 = (bf16[128,128]{1,0:T(8,128)(2,1)S(1)}, bf16[128,128]{1,0:T(8,128)(2,1)}, u32[]{:S(2)}) copy-start(bf16[128,128]{1,0:T(8,128)(2,1)} %outer_ref.1) | copy-start | bytes 98308
  7.3 35.1 %all-to-all-start = ((bf16[32,24,128]{2,1,0:T(8,128)(2,1)}), bf16[32,24,128]{2,1,0:T(8,128)(2,1)S(1)}, u32[]{:S(2)}, u32[]{:S(2)}) async-start(bf16[32,24,128]{2,1,0:T(8,128)(2,1)} %bitcast.18), calls=%async_computation | async-start | bytes 393216 | tf_op jit(solution)/shard_map/all_to_all | solution.py:28
  23.7 28.4 %collective-permute-start.2 = (bf16[2048,256]{1,0:T(8,128)(2,1)S(1)}, bf16[2048,256]{1,0:T(8,128)(2,1)}, u32[]{:S(2)}, u32[]{:S(2)}) collective-permute-start(bf16[2048,256]{1,0:T(8,128)(2,1)S(1)} %get-tuple-element.17.own_ref), channel_id=1, source_target_pairs={{0,12},{4,0},{8,4},{12,8},{1,13},{5,1},{9,5},{13,9},{2,14},{6,2},{... | collective-permute-start | bytes 3145736 | tf_op jit(solution)/shard_map/ppermute | solution.py:24
  27.0 34.8 %collective-permute-start.3 = (bf16[2048,256]{1,0:T(8,128)(2,1)S(1)}, bf16[2048,256]{1,0:T(8,128)(2,1)}, u32[]{:S(2)}, u32[]{:S(2)}) collective-permute-start(bf16[2048,256]{1,0:T(8,128)(2,1)S(1)} %collective-permute-done.1.w1_ref), channel_id=1, source_target_pairs={{0,4},{4,8},{8,12},{12,0},{1,5},{5,9},{9,13},{13,1},{2,6},{6,10},{... | collective-permute-start | bytes 3145736 | tf_op jit(solution)/shard_map/ppermute | solution.py:24
  34.9 6.8 %collective-permute-start = (bf16[2,128]{1,0:T(2,128)(2,1)S(1)}, bf16[2,128]{1,0:T(2,128)(2,1)S(1)}, u32[]{:S(2)}, u32[]{:S(2)}) collective-permute-start(bf16[2,128]{1,0:T(2,128)(2,1)S(1)} %get-tuple-element.14), channel_id=1, source_target_pairs={{0,16},{16,32},{32,48},{48,64},{64,80},{80,96},{96,112},{112,128},... | collective-permute-start | bytes 1544 | tf_op jit(solution)/shard_map/ppermute | solution.py:19
  44.3 17.5 %all-to-all-start.1 = ((bf16[4,1024,128]{2,1,0:T(8,128)(2,1)}), bf16[4,1024,128]{2,1,0:T(8,128)(2,1)S(1)}, u32[]{:S(2)}, u32[]{:S(2)}) async-start(bf16[4,1024,128]{2,1,0:T(8,128)(2,1)} %copies.1), calls=%async_computation.1 | async-start | bytes 2097152 | tf_op jit(solution)/shard_map/all_to_all | solution.py:28
  48.3 23.9 %collective-permute-start.5 = (bf16[1,2048,128]{2,1,0:T(8,128)(2,1)}, bf16[1,2048,128]{2,1,0:T(8,128)(2,1)}, u32[]{:S(2)}, u32[]{:S(2)}) collective-permute-start(bf16[1,2048,128]{2,1,0:T(8,128)(2,1)} %w0_ref.1), channel_id=1, source_target_pairs={{0,12},{4,0},{8,4},{12,8},{1,13},{5,1},{9,5},{13,9},{2,14},{6,2},{... | collective-permute-start | bytes 1572872 | tf_op jit(solution)/shard_map/ppermute | solution.py:24
  65.3 19.6 %all-to-all-start.2 = ((bf16[4,192,512]{2,1,0:T(8,128)(2,1)}), bf16[4,192,512]{2,1,0:T(8,128)(2,1)S(1)}, u32[]{:S(2)}, u32[]{:S(2)}) async-start(bf16[4,192,512]{2,1,0:T(8,128)(2,1)} %get-tuple-element.18), calls=%async_computation.2 | async-start | bytes 1572864 | tf_op jit(solution)/shard_map/all_to_all | solution.py:28
  68.9 14.0 %collective-permute-start.4 = (bf16[1,2048,128]{2,1,0:T(8,128)(2,1)S(1)}, bf16[1,2048,128]{2,1,0:T(8,128)(2,1)S(1)}, u32[]{:S(2)}, u32[]{:S(2)}) collective-permute-start(bf16[1,2048,128]{2,1,0:T(8,128)(2,1)S(1)} %copy-done.3), channel_id=1, source_target_pairs={{0,4},{4,8},{8,12},{12,0},{1,5},{5,9},{9,13},{13,1},{2,6},{6,10},{... | collective-permute-start | bytes 1572872 | tf_op jit(solution)/shard_map/ppermute | solution.py:24
  72.1 12.7 %collective-permute-start.6 = (bf16[1,2048,128]{2,1,0:T(8,128)(2,1)}, bf16[1,2048,128]{2,1,0:T(8,128)(2,1)S(1)}, u32[]{:S(2)}, u32[]{:S(2)}) collective-permute-start(bf16[1,2048,128]{2,1,0:T(8,128)(2,1)} %collective-permute-done.5.w2_ref), channel_id=1, source_target_pairs={{0,12},{4,0},{8,4},{12,8},{1,13},{5,1},{9,5},{13,9},{2,14},{6,2},{... | collective-permute-start | bytes 1572872 | tf_op jit(solution)/shard_map/ppermute | solution.py:24
  88.5 32.6 %copy-start.10 = (f32[128,4]{0,1:T(4,128)S(1)}, f32[128,4]{0,1:T(4,128)}, u32[]{:S(2)}) copy-start(f32[128,4]{0,1:T(4,128)} %param.27) | copy-start | bytes 6148
  88.5 32.6 %copy-start.9 = (s32[128,4]{0,1:T(4,128)S(1)}, s32[128,4]{0,1:T(4,128)}, u32[]{:S(2)}) copy-start(s32[128,4]{0,1:T(4,128)} %param.26) | copy-start | bytes 6148
  88.5 42.2 %copy-start.5 = (bf16[2048,128]{1,0:T(8,128)(2,1)S(1)}, bf16[2048,128]{1,0:T(8,128)(2,1)}, u32[]{:S(2)}) copy-start(bf16[2048,128]{1,0:T(8,128)(2,1)} %shared_ref.1) | copy-start | bytes 1572868
  88.5 45.8 %all-to-all-start.3 = ((bf16[128,8,128]{2,1,0:T(8,128)(2,1)}), bf16[128,8,128]{2,1,0:T(8,128)(2,1)S(1)}, u32[]{:S(2)}, u32[]{:S(2)}) async-start(bf16[128,8,128]{2,1,0:T(8,128)(2,1)} %bitcast.15), calls=%async_computation.3 | async-start | bytes 524288 | tf_op jit(solution)/shard_map/all_to_all | solution.py:28
  110.9 19.8 %copy-start.4 = (bf16[2048,128]{1,0:T(8,128)(2,1)S(1)}, bf16[2048,128]{1,0:T(8,128)(2,1)}, u32[]{:S(2)}) copy-start(bf16[2048,128]{1,0:T(8,128)(2,1)} %mix_ref.1) | copy-start | bytes 1572868
  111.0 11.7 %collective-permute-start.7 = (bf16[4,256,128]{2,1,0:T(8,128)(2,1)S(1)}, bf16[4,256,128]{2,1,0:T(8,128)(2,1)S(1)}, u32[]{:S(2)}, u32[]{:S(2)}) collective-permute-start(bf16[4,256,128]{2,1,0:T(8,128)(2,1)S(1)} %get-tuple-element.19.own_ref), channel_id=1, source_target_pairs={{0,4},{4,8},{8,12},{12,0},{1,5},{5,9},{9,13},{13,1},{2,6},{6,10},{... | collective-permute-start | bytes 786440 | tf_op jit(solution)/shard_map/ppermute | solution.py:24
  114.4 10.6 %collective-permute-start.8 = (bf16[4,256,128]{2,1,0:T(8,128)(2,1)S(1)}, bf16[4,256,128]{2,1,0:T(8,128)(2,1)S(1)}, u32[]{:S(2)}, u32[]{:S(2)}) collective-permute-start(bf16[4,256,128]{2,1,0:T(8,128)(2,1)S(1)} %get-tuple-element.19.own_ref), channel_id=1, source_target_pairs={{0,12},{4,0},{8,4},{12,8},{1,13},{5,1},{9,5},{13,9},{2,14},{6,2},{... | collective-permute-start | bytes 786440 | tf_op jit(solution)/shard_map/ppermute | solution.py:24
  117.6 13.2 %collective-permute-start.9 = (bf16[4,256,128]{2,1,0:T(8,128)(2,1)S(1)}, bf16[4,256,128]{2,1,0:T(8,128)(2,1)S(1)}, u32[]{:S(2)}, u32[]{:S(2)}) collective-permute-start(bf16[4,256,128]{2,1,0:T(8,128)(2,1)S(1)} %get-tuple-element.19.own_ref), channel_id=1, source_target_pairs={{0,8},{4,12},{8,0},{12,4},{1,9},{5,13},{9,1},{13,5},{2,10},{6,14},... | collective-permute-start | bytes 786440 | tf_op jit(solution)/shard_map/ppermute | solution.py:24
  134.4 6.8 %copy-start.15 = (bf16[128]{0:T(256)(128)(2,1)S(1)}, bf16[128]{0:T(256)(128)(2,1)}, u32[]{:S(2)}) copy-start(bf16[128]{0:T(256)(128)(2,1)} %param.23) | copy-start | bytes 772
  135.5 12.1 %all-to-all-start.4 = ((f32[16,4,128]{2,1,0:T(4,128)}), f32[16,4,128]{2,1,0:T(4,128)S(1)}, u32[]{:S(2)}, u32[]{:S(2)}) async-start(f32[16,4,128]{2,1,0:T(4,128)} %get-tuple-element.22), calls=%async_computation.4 | async-start | bytes 65536 | tf_op jit(solution)/shard_map/all_to_all | solution.py:28
  (7 other events, 8.4 us)

commit v3 on v2

--- a/solution.py
+++ b/solution.py
@@ -127,7 +127,10 @@
     )(*far(ids, x, gate, up))
 
 
-def front_kernel(inner_ref, value_ref, x_ref, gate_ref, up_ref, product_ref, tail_ref, hidden_ref):
+def front_kernel(
+    inner_ref, value_ref, x_ref, gate_ref, up_ref, taps_ref, product_ref, tail_ref, hidden_ref, wide_ref
+):
+    wide_ref[...] = taps_ref[...].astype(F32)
     product = (inner_ref[...].astype(F32) * value_ref[...].astype(F32)).astype(BF16)
     product_ref[...] = product
     tail_ref[...] = product[126:128]
@@ -145,9 +148,10 @@
             pltpu.VMEM((128, 128), BF16),
             pltpu.VMEM((2, 128), BF16),
             pltpu.VMEM((128, 128), BF16),
+            pltpu.VMEM((3, 128), F32),
         ],
-        in_specs=vmem(5),
-        out_specs=vmem(3),
+        in_specs=vmem(6),
+        out_specs=vmem(4),
     )(*arrays)
 
 
@@ -156,7 +160,7 @@
     rows_ref[8:136, :] = product_ref[...].astype(F32)
     convolved = jnp.zeros((128, 128), F32)
     for tap in range(3):
-        convolved = convolved + taps_ref[tap : tap + 1, :].astype(F32) * rows_ref[6 + tap : 134 + tap, :]
+        convolved = convolved + taps_ref[tap : tap + 1, :] * rows_ref[6 + tap : 134 + tap, :]
     weighted = (outer_ref[...].astype(F32) * convolved).astype(BF16)
     for q in range(4):
         out_ref[q, 0:768, :] = a_ref[...]
@@ -173,7 +177,7 @@
         in_specs=vmem(6),
         out_specs=vmem(1)[0],
         scratch_shapes=[pltpu.VMEM((136, 128), F32)],
-    )(*near(arrived, border, product), outer, taps, *near(shared))
+    )(*near(arrived, border, product), outer, *near(taps, shared))
 
 
 def hidden_kernel(x_ref, own_ref, w1_ref, w2_ref, w3_ref, out_ref, rest_ref, wide_ref, rows_ref):
@@ -375,11 +379,11 @@
     down1, down2 = rotated(expert_down, 1), rotated(expert_down, -1)
     down3 = rotated(down2, -1)
 
-    product, tail, shared_hidden = front(
-        inner_gate, conv_value, moe_input, shared_gate, shared_up
+    product, tail, shared_hidden, taps = front(
+        inner_gate, conv_value, moe_input, shared_gate, shared_up, conv_taps
     )
     border = shifted(tail, "ep", 1)
-    rows = copies(arrived, border, product, outer_gate, conv_taps, shared_hidden)
+    rows = copies(arrived, border, product, outer_gate, taps, shared_hidden)
     rows = exchanged(rows, "x")
     hidden, wide = hidden_of(rows, own, before, after, beyond)
     hidden = exchanged(hidden, "x")

time: 149 us -> 149 us (level)
  no operation moved by 1% of the time
where the time goes in v3:
time: 149 us; the launch traced here: 148 us
  starting transfers between devices  91.3 us (61%)
  waiting for transfers between devices  38.3 us (26%)
  Pallas kernels  14.3 us (10%)
  local copies, waits for them, and re-layouts  2.79 us (2%)
    all_to_all x5, starting transfers between devices, exchanged(): return lax.all_to_all(x, axis, split_axis=0, concat_axis=0, tiled=True)  52 us
    ppermute x9, starting transfers between devices, rotated(): lax.ppermute(x, 'y', [(i, (i + distance) % count) for i in range(count)])  33.1 us
    all_to_all x5, waiting for transfers between devices, exchanged(): return lax.all_to_all(x, axis, split_axis=0, concat_axis=0, tiled=True)  19.3 us
    ppermute x9, waiting for transfers between devices, rotated(): lax.ppermute(x, 'y', [(i, (i + distance) % count) for i in range(count)])  18.4 us
    ppermute x1, starting transfers between devices, shifted(): return lax.ppermute(block, axis, route)  6.14 us
    pallas_call x1, Pallas kernels, down_of(): pl.pallas_call(down_kernel, name='down', compiler_params=LIMIT, out_shape...  3.66 us
    pallas_call x1, Pallas kernels, hidden_of(): pl.pallas_call(hidden_kernel, name='hidden', compiler_params=LIMIT, out_s...  3.54 us
  transfers between devices with their start and end apart: 15, of which 10 were waited for; matrix products, arithmetic and copies ran while one was open for 0% of the time, Pallas kernels for 4%

profile of v3, /device:TPU:1, one launch (start us, length us, event | category | flops | bytes accessed | tf_op | source)
XLA Modules:
  0.0 147.7 jit_solution(9192162394328067916)
XLA Ops:
  0.6 2.6 %pack.1 = (bf16[768,128]{1,0:T(8,128)(2,1)}, bf16[2048,256]{1,0:T(8,128)(2,1)S(1)}) custom-call(s32[4,128]{1,0:T(4,128)} %bitcast.12, bf16[128,2048]{1,0:T(8,128)(2,1)} %x_ref.1, bf16[2048,128]{1,0:T(8,128)(2,1)} %bitcast.16, bf16[2048,128]{1,0:T(8,128)(2,1)} %bitcast.17), custom_call_target="tpu_custom_call" | custom-call | tf_op jit(solution)/shard_map/pack/pallas_call | solution.py:113
  3.3 4.0 %collective-permute-start.1 = (bf16[2048,256]{1,0:T(8,128)(2,1)S(1)}, bf16[2048,256]{1,0:T(8,128)(2,1)S(1)}, u32[]{:S(2)}, u32[]{:S(2)}) collective-permute-start(bf16[2048,256]{1,0:T(8,128)(2,1)S(1)} %get-tuple-element.19.own_ref), channel_id=1, source_target_pairs={{0,4},{4,8},{8,12},{12,0},{1,5},{5,9},{9,13},{13,1},{2,6},{6,10},{... | collective-permute-start | bytes 3145736 | tf_op jit(solution)/shard_map/ppermute | solution.py:24
  7.3 16.3 %all-to-all-start = ((bf16[32,24,128]{2,1,0:T(8,128)(2,1)}), bf16[32,24,128]{2,1,0:T(8,128)(2,1)S(1)}, u32[]{:S(2)}, u32[]{:S(2)}) async-start(bf16[32,24,128]{2,1,0:T(8,128)(2,1)} %bitcast.18), calls=%async_computation | async-start | bytes 393216 | tf_op jit(solution)/shard_map/all_to_all | solution.py:28
  23.7 3.3 %collective-permute-start.2 = (bf16[2048,256]{1,0:T(8,128)(2,1)S(1)}, bf16[2048,256]{1,0:T(8,128)(2,1)}, u32[]{:S(2)}, u32[]{:S(2)}) collective-permute-start(bf16[2048,256]{1,0:T(8,128)(2,1)S(1)} %get-tuple-element.19.own_ref), channel_id=1, source_target_pairs={{0,12},{4,0},{8,4},{12,8},{1,13},{5,1},{9,5},{13,9},{2,14},{6,2},{... | collective-permute-start | bytes 3145736 | tf_op jit(solution)/shard_map/ppermute | solution.py:24
  27.0 5.3 %collective-permute-start.3 = (bf16[2048,256]{1,0:T(8,128)(2,1)S(1)}, bf16[2048,256]{1,0:T(8,128)(2,1)}, u32[]{:S(2)}, u32[]{:S(2)}) collective-permute-start(bf16[2048,256]{1,0:T(8,128)(2,1)S(1)} %collective-permute-done.1.w1_ref), channel_id=1, source_target_pairs={{0,4},{4,8},{8,12},{12,0},{1,5},{5,9},{9,13},{13,1},{2,6},{6,10},{... | collective-permute-start | bytes 3145736 | tf_op jit(solution)/shard_map/ppermute | solution.py:24
  34.9 6.1 %collective-permute-start = (bf16[2,128]{1,0:T(2,128)(2,1)S(1)}, bf16[2,128]{1,0:T(2,128)(2,1)S(1)}, u32[]{:S(2)}, u32[]{:S(2)}) collective-permute-start(bf16[2,128]{1,0:T(2,128)(2,1)S(1)} %get-tuple-element.15), channel_id=1, source_target_pairs={{0,16},{16,32},{32,48},{48,64},{64,80},{80,96},{96,112},{112,128},... | collective-permute-start | bytes 1544 | tf_op jit(solution)/shard_map/ppermute | solution.py:19
  43.6 4.0 %all-to-all-start.1 = ((bf16[4,1024,128]{2,1,0:T(8,128)(2,1)}), bf16[4,1024,128]{2,1,0:T(8,128)(2,1)S(1)}, u32[]{:S(2)}, u32[]{:S(2)}) async-start(bf16[4,1024,128]{2,1,0:T(8,128)(2,1)} %copies.1), calls=%async_computation.1 | async-start | bytes 2097152 | tf_op jit(solution)/shard_map/all_to_all | solution.py:28
  47.6 3.8 %collective-permute-start.5 = (bf16[1,2048,128]{2,1,0:T(8,128)(2,1)}, bf16[1,2048,128]{2,1,0:T(8,128)(2,1)}, u32[]{:S(2)}, u32[]{:S(2)}) collective-permute-start(bf16[1,2048,128]{2,1,0:T(8,128)(2,1)} %w0_ref.1), channel_id=1, source_target_pairs={{0,12},{4,0},{8,4},{12,8},{1,13},{5,1},{9,5},{13,9},{2,14},{6,2},{... | collective-permute-start | bytes 1572872 | tf_op jit(solution)/shard_map/ppermute | solution.py:24
  51.5 9.6 %all-to-all-done.1.x_ref = bf16[4,1024,128]{2,1,0:T(8,128)(2,1)S(1)} async-done(((bf16[4,1024,128]{2,1,0:T(8,128)(2,1)}), bf16[4,1024,128]{2,1,0:T(8,128)(2,1)S(1)}, u32[]{:S(2)}, u32[]{:S(2)}) %all-to-all-start.1) | async-done | bytes 1048608 | tf_op jit(solution)/shard_map/all_to_all | solution.py:28
  61.1 3.5 %hidden.1 = (bf16[4,192,512]{2,1,0:T(8,128)(2,1)}, bf16[4,256,128]{2,1,0:T(8,128)(2,1)S(1)}) custom-call(bf16[4,1024,128]{2,1,0:T(8,128)(2,1)S(1)} %all-to-all-done.1.x_ref, bf16[2048,256]{1,0:T(8,128)(2,1)S(1)} %get-tuple-element.19.own_ref, bf16[2048,256]{1,0:T(8,128)(2,1)S(1)} %collective-permute-done.1.w1_ref, ...), custom_call_target="tpu_custom_call" | custom-call | tf_op jit(solution)/shard_map/hidden/pallas_call | solution.py:200
  64.6 3.6 %all-to-all-start.2 = ((bf16[4,192,512]{2,1,0:T(8,128)(2,1)}), bf16[4,192,512]{2,1,0:T(8,128)(2,1)S(1)}, u32[]{:S(2)}, u32[]{:S(2)}) async-start(bf16[4,192,512]{2,1,0:T(8,128)(2,1)} %get-tuple-element.20), calls=%async_computation.2 | async-start | bytes 1572864 | tf_op jit(solution)/shard_map/all_to_all | solution.py:28
  68.3 3.2 %collective-permute-start.4 = (bf16[1,2048,128]{2,1,0:T(8,128)(2,1)S(1)}, bf16[1,2048,128]{2,1,0:T(8,128)(2,1)S(1)}, u32[]{:S(2)}, u32[]{:S(2)}) collective-permute-start(bf16[1,2048,128]{2,1,0:T(8,128)(2,1)S(1)} %copy-done.3), channel_id=1, source_target_pairs={{0,4},{4,8},{8,12},{12,0},{1,5},{5,9},{9,13},{13,1},{2,6},{6,10},{... | collective-permute-start | bytes 1572872 | tf_op jit(solution)/shard_map/ppermute | solution.py:24
  71.5 3.3 %collective-permute-start.6 = (bf16[1,2048,128]{2,1,0:T(8,128)(2,1)}, bf16[1,2048,128]{2,1,0:T(8,128)(2,1)S(1)}, u32[]{:S(2)}, u32[]{:S(2)}) collective-permute-start(bf16[1,2048,128]{2,1,0:T(8,128)(2,1)} %collective-permute-done.5.w2_ref), channel_id=1, source_target_pairs={{0,12},{4,0},{8,4},{12,8},{1,13},{5,1},{9,5},{13,9},{2,14},{6,2},{... | collective-permute-start | bytes 1572872 | tf_op jit(solution)/shard_map/ppermute | solution.py:24
  74.8 7.5 %collective-permute-done.4.w1_ref = bf16[1,2048,128]{2,1,0:T(8,128)(2,1)S(1)} collective-permute-done((bf16[1,2048,128]{2,1,0:T(8,128)(2,1)S(1)}, bf16[1,2048,128]{2,1,0:T(8,128)(2,1)S(1)}, u32[]{:S(2)}, u32[]{:S(2)}) %collective-permute-start.4) | collective-permute-done | bytes 524320 | tf_op jit(solution)/shard_map/ppermute | solution.py:24
  84.2 3.7 %down.1 = bf16[32,4,8,128]{3,2,1,0:T(8,128)(2,1)} custom-call(bf16[4,192,512]{2,1,0:T(8,128)(2,1)S(1)} %all-to-all-done.2.h_ref, bf16[1,2048,128]{2,1,0:T(8,128)(2,1)S(1)} %copy-done.3, bf16[1,2048,128]{2,1,0:T(8,128)(2,1)S(1)} %collective-permute-done.4.w1_ref, bf16[1,2048,128]{2,1,0:T(8,128)(2,1)} %collective-permute-done.5.w2_ref, ...), custom_call_target="tpu_custom_call" | custom-call | tf_op jit(solution)/shard_map/down/pallas_call | solution.py:228
  87.9 22.4 %all-to-all-start.3 = ((bf16[128,8,128]{2,1,0:T(8,128)(2,1)}), bf16[128,8,128]{2,1,0:T(8,128)(2,1)S(1)}, u32[]{:S(2)}, u32[]{:S(2)}) async-start(bf16[128,8,128]{2,1,0:T(8,128)(2,1)} %bitcast.15), calls=%async_computation.3 | async-start | bytes 524288 | tf_op jit(solution)/shard_map/all_to_all | solution.py:28
  110.3 3.4 %collective-permute-start.7 = (bf16[4,256,128]{2,1,0:T(8,128)(2,1)S(1)}, bf16[4,256,128]{2,1,0:T(8,128)(2,1)S(1)}, u32[]{:S(2)}, u32[]{:S(2)}) collective-permute-start(bf16[4,256,128]{2,1,0:T(8,128)(2,1)S(1)} %get-tuple-element.21.own_ref), channel_id=1, source_target_pairs={{0,4},{4,8},{8,12},{12,0},{1,5},{5,9},{9,13},{13,1},{2,6},{6,10},{... | collective-permute-start | bytes 786440 | tf_op jit(solution)/shard_map/ppermute | solution.py:24
  113.7 3.2 %collective-permute-start.8 = (bf16[4,256,128]{2,1,0:T(8,128)(2,1)S(1)}, bf16[4,256,128]{2,1,0:T(8,128)(2,1)S(1)}, u32[]{:S(2)}, u32[]{:S(2)}) collective-permute-start(bf16[4,256,128]{2,1,0:T(8,128)(2,1)S(1)} %get-tuple-element.21.own_ref), channel_id=1, source_target_pairs={{0,12},{4,0},{8,4},{12,8},{1,13},{5,1},{9,5},{13,9},{2,14},{6,2},{... | collective-permute-start | bytes 786440 | tf_op jit(solution)/shard_map/ppermute | solution.py:24
  116.9 3.6 %collective-permute-start.9 = (bf16[4,256,128]{2,1,0:T(8,128)(2,1)S(1)}, bf16[4,256,128]{2,1,0:T(8,128)(2,1)S(1)}, u32[]{:S(2)}, u32[]{:S(2)}) collective-permute-start(bf16[4,256,128]{2,1,0:T(8,128)(2,1)S(1)} %get-tuple-element.21.own_ref), channel_id=1, source_target_pairs={{0,8},{4,12},{8,0},{12,4},{1,9},{5,13},{9,1},{13,5},{2,10},{6,14},... | collective-permute-start | bytes 786440 | tf_op jit(solution)/shard_map/ppermute | solution.py:24
  121.9 2.4 %collective-permute-done.8.n2_ref = bf16[4,256,128]{2,1,0:T(8,128)(2,1)S(1)} collective-permute-done((bf16[4,256,128]{2,1,0:T(8,128)(2,1)S(1)}, bf16[4,256,128]{2,1,0:T(8,128)(2,1)S(1)}, u32[]{:S(2)}, u32[]{:S(2)}) %collective-permute-start.8) | collective-permute-done | bytes 262176 | tf_op jit(solution)/shard_map/ppermute | solution.py:24
  124.3 5.8 %collective-permute-done.9.n3_ref = bf16[4,256,128]{2,1,0:T(8,128)(2,1)S(1)} collective-permute-done((bf16[4,256,128]{2,1,0:T(8,128)(2,1)S(1)}, bf16[4,256,128]{2,1,0:T(8,128)(2,1)S(1)}, u32[]{:S(2)}, u32[]{:S(2)}) %collective-permute-start.9) | collective-permute-done | bytes 262176 | tf_op jit(solution)/shard_map/ppermute | solution.py:24
  130.6 3.2 %all-to-all-done.3.back_ref = bf16[128,8,128]{2,1,0:T(8,128)(2,1)S(1)} async-done(((bf16[128,8,128]{2,1,0:T(8,128)(2,1)}), bf16[128,8,128]{2,1,0:T(8,128)(2,1)S(1)}, u32[]{:S(2)}, u32[]{:S(2)}) %all-to-all-start.3) | async-done | bytes 262176 | tf_op jit(solution)/shard_map/all_to_all | solution.py:28
  134.8 5.6 %all-to-all-start.4 = ((f32[16,4,128]{2,1,0:T(4,128)}), f32[16,4,128]{2,1,0:T(4,128)S(1)}, u32[]{:S(2)}, u32[]{:S(2)}) async-start(f32[16,4,128]{2,1,0:T(4,128)} %get-tuple-element.24), calls=%async_computation.4 | async-start | bytes 65536 | tf_op jit(solution)/shard_map/all_to_all | solution.py:28
  141.2 5.7 %all-to-all-done.4.stats_ref = f32[16,4,128]{2,1,0:T(4,128)S(1)} async-done(((f32[16,4,128]{2,1,0:T(4,128)}), f32[16,4,128]{2,1,0:T(4,128)S(1)}, u32[]{:S(2)}, u32[]{:S(2)}) %all-to-all-start.4) | async-done | bytes 32800 | tf_op jit(solution)/shard_map/all_to_all | solution.py:28
  (48 shorter events, 11.5 us)
Async XLA Ops:
  0.6 31.7 %copy-start = (bf16[128,2048]{1,0:T(8,128)(2,1)S(1)}, bf16[128,2048]{1,0:T(8,128)(2,1)}, u32[]{:S(2)}) copy-start(bf16[128,2048]{1,0:T(8,128)(2,1)} %x_ref.1) | copy-start | bytes 1572868
  3.3 23.7 %collective-permute-start.1 = (bf16[2048,256]{1,0:T(8,128)(2,1)S(1)}, bf16[2048,256]{1,0:T(8,128)(2,1)S(1)}, u32[]{:S(2)}, u32[]{:S(2)}) collective-permute-start(bf16[2048,256]{1,0:T(8,128)(2,1)S(1)} %get-tuple-element.19.own_ref), channel_id=1, source_target_pairs={{0,4},{4,8},{8,12},{12,0},{1,5},{5,9},{9,13},{13,1},{2,6},{6,10},{... | collective-permute-start | bytes 3145736 | tf_op jit(solution)/shard_map/ppermute | solution.py:24
  7.3 25.0 %copy-start.6 = (bf16[128,128]{1,0:T(8,128)(2,1)S(1)}, bf16[128,128]{1,0:T(8,128)(2,1)}, u32[]{:S(2)}) copy-start(bf16[128,128]{1,0:T(8,128)(2,1)} %inner_ref.1) | copy-start | bytes 98308
  7.3 25.0 %copy-start.7 = (bf16[128,128]{1,0:T(8,128)(2,1)S(1)}, bf16[128,128]{1,0:T(8,128)(2,1)}, u32[]{:S(2)}) copy-start(bf16[128,128]{1,0:T(8,128)(2,1)} %value_ref.1) | copy-start | bytes 98308
  7.3 25.0 %copy-start.11 = (bf16[3,128]{1,0:T(4,128)(2,1)S(1)}, bf16[3,128]{1,0:T(4,128)(2,1)}, u32[]{:S(2)}) copy-start(bf16[3,128]{1,0:T(4,128)(2,1)} %taps_ref.1) | copy-start | bytes 2308
  7.3 35.2 %copy-start.8 = (bf16[128,128]{1,0:T(8,128)(2,1)S(1)}, bf16[128,128]{1,0:T(8,128)(2,1)}, u32[]{:S(2)}) copy-start(bf16[128,128]{1,0:T(8,128)(2,1)} %outer_ref.1) | copy-start | bytes 98308
  7.3 35.1 %all-to-all-start = ((bf16[32,24,128]{2,1,0:T(8,128)(2,1)}), bf16[32,24,128]{2,1,0:T(8,128)(2,1)S(1)}, u32[]{:S(2)}, u32[]{:S(2)}) async-start(bf16[32,24,128]{2,1,0:T(8,128)(2,1)} %bitcast.18), calls=%async_computation | async-start | bytes 393216 | tf_op jit(solution)/shard_map/all_to_all | solution.py:28
  23.7 27.7 %collective-permute-start.2 = (bf16[2048,256]{1,0:T(8,128)(2,1)S(1)}, bf16[2048,256]{1,0:T(8,128)(2,1)}, u32[]{:S(2)}, u32[]{:S(2)}) collective-permute-start(bf16[2048,256]{1,0:T(8,128)(2,1)S(1)} %get-tuple-element.19.own_ref), channel_id=1, source_target_pairs={{0,12},{4,0},{8,4},{12,8},{1,13},{5,1},{9,5},{13,9},{2,14},{6,2},{... | collective-permute-start | bytes 3145736 | tf_op jit(solution)/shard_map/ppermute | solution.py:24
  27.0 34.1 %collective-permute-start.3 = (bf16[2048,256]{1,0:T(8,128)(2,1)S(1)}, bf16[2048,256]{1,0:T(8,128)(2,1)}, u32[]{:S(2)}, u32[]{:S(2)}) collective-permute-start(bf16[2048,256]{1,0:T(8,128)(2,1)S(1)} %collective-permute-done.1.w1_ref), channel_id=1, source_target_pairs={{0,4},{4,8},{8,12},{12,0},{1,5},{5,9},{9,13},{13,1},{2,6},{6,10},{... | collective-permute-start | bytes 3145736 | tf_op jit(solution)/shard_map/ppermute | solution.py:24
  34.9 6.8 %collective-permute-start = (bf16[2,128]{1,0:T(2,128)(2,1)S(1)}, bf16[2,128]{1,0:T(2,128)(2,1)S(1)}, u32[]{:S(2)}, u32[]{:S(2)}) collective-permute-start(bf16[2,128]{1,0:T(2,128)(2,1)S(1)} %get-tuple-element.15), channel_id=1, source_target_pairs={{0,16},{16,32},{32,48},{48,64},{64,80},{80,96},{96,112},{112,128},... | collective-permute-start | bytes 1544 | tf_op jit(solution)/shard_map/ppermute | solution.py:19
  43.6 17.5 %all-to-all-start.1 = ((bf16[4,1024,128]{2,1,0:T(8,128)(2,1)}), bf16[4,1024,128]{2,1,0:T(8,128)(2,1)S(1)}, u32[]{:S(2)}, u32[]{:S(2)}) async-start(bf16[4,1024,128]{2,1,0:T(8,128)(2,1)} %copies.1), calls=%async_computation.1 | async-start | bytes 2097152 | tf_op jit(solution)/shard_map/all_to_all | solution.py:28
  47.6 23.9 %collective-permute-start.5 = (bf16[1,2048,128]{2,1,0:T(8,128)(2,1)}, bf16[1,2048,128]{2,1,0:T(8,128)(2,1)}, u32[]{:S(2)}, u32[]{:S(2)}) collective-permute-start(bf16[1,2048,128]{2,1,0:T(8,128)(2,1)} %w0_ref.1), channel_id=1, source_target_pairs={{0,12},{4,0},{8,4},{12,8},{1,13},{5,1},{9,5},{13,9},{2,14},{6,2},{... | collective-permute-start | bytes 1572872 | tf_op jit(solution)/shard_map/ppermute | solution.py:24
  64.6 19.6 %all-to-all-start.2 = ((bf16[4,192,512]{2,1,0:T(8,128)(2,1)}), bf16[4,192,512]{2,1,0:T(8,128)(2,1)S(1)}, u32[]{:S(2)}, u32[]{:S(2)}) async-start(bf16[4,192,512]{2,1,0:T(8,128)(2,1)} %get-tuple-element.20), calls=%async_computation.2 | async-start | bytes 1572864 | tf_op jit(solution)/shard_map/all_to_all | solution.py:28
  68.3 14.0 %collective-permute-start.4 = (bf16[1,2048,128]{2,1,0:T(8,128)(2,1)S(1)}, bf16[1,2048,128]{2,1,0:T(8,128)(2,1)S(1)}, u32[]{:S(2)}, u32[]{:S(2)}) collective-permute-start(bf16[1,2048,128]{2,1,0:T(8,128)(2,1)S(1)} %copy-done.3), channel_id=1, source_target_pairs={{0,4},{4,8},{8,12},{12,0},{1,5},{5,9},{9,13},{13,1},{2,6},{6,10},{... | collective-permute-start | bytes 1572872 | tf_op jit(solution)/shard_map/ppermute | solution.py:24
  71.5 12.7 %collective-permute-start.6 = (bf16[1,2048,128]{2,1,0:T(8,128)(2,1)}, bf16[1,2048,128]{2,1,0:T(8,128)(2,1)S(1)}, u32[]{:S(2)}, u32[]{:S(2)}) collective-permute-start(bf16[1,2048,128]{2,1,0:T(8,128)(2,1)} %collective-permute-done.5.w2_ref), channel_id=1, source_target_pairs={{0,12},{4,0},{8,4},{12,8},{1,13},{5,1},{9,5},{13,9},{2,14},{6,2},{... | collective-permute-start | bytes 1572872 | tf_op jit(solution)/shard_map/ppermute | solution.py:24
  87.9 32.6 %copy-start.10 = (f32[128,4]{0,1:T(4,128)S(1)}, f32[128,4]{0,1:T(4,128)}, u32[]{:S(2)}) copy-start(f32[128,4]{0,1:T(4,128)} %param.27) | copy-start | bytes 6148
  87.9 32.7 %copy-start.9 = (s32[128,4]{0,1:T(4,128)S(1)}, s32[128,4]{0,1:T(4,128)}, u32[]{:S(2)}) copy-start(s32[128,4]{0,1:T(4,128)} %param.26) | copy-start | bytes 6148
  87.9 42.2 %copy-start.5 = (bf16[2048,128]{1,0:T(8,128)(2,1)S(1)}, bf16[2048,128]{1,0:T(8,128)(2,1)}, u32[]{:S(2)}) copy-start(bf16[2048,128]{1,0:T(8,128)(2,1)} %shared_ref.1) | copy-start | bytes 1572868
  87.9 45.8 %all-to-all-start.3 = ((bf16[128,8,128]{2,1,0:T(8,128)(2,1)}), bf16[128,8,128]{2,1,0:T(8,128)(2,1)S(1)}, u32[]{:S(2)}, u32[]{:S(2)}) async-start(bf16[128,8,128]{2,1,0:T(8,128)(2,1)} %bitcast.15), calls=%async_computation.3 | async-start | bytes 524288 | tf_op jit(solution)/shard_map/all_to_all | solution.py:28
  110.3 19.8 %copy-start.4 = (bf16[2048,128]{1,0:T(8,128)(2,1)S(1)}, bf16[2048,128]{1,0:T(8,128)(2,1)}, u32[]{:S(2)}) copy-start(bf16[2048,128]{1,0:T(8,128)(2,1)} %mix_ref.1) | copy-start | bytes 1572868
  110.3 11.7 %collective-permute-start.7 = (bf16[4,256,128]{2,1,0:T(8,128)(2,1)S(1)}, bf16[4,256,128]{2,1,0:T(8,128)(2,1)S(1)}, u32[]{:S(2)}, u32[]{:S(2)}) collective-permute-start(bf16[4,256,128]{2,1,0:T(8,128)(2,1)S(1)} %get-tuple-element.21.own_ref), channel_id=1, source_target_pairs={{0,4},{4,8},{8,12},{12,0},{1,5},{5,9},{9,13},{13,1},{2,6},{6,10},{... | collective-permute-start | bytes 786440 | tf_op jit(solution)/shard_map/ppermute | solution.py:24
  113.7 10.6 %collective-permute-start.8 = (bf16[4,256,128]{2,1,0:T(8,128)(2,1)S(1)}, bf16[4,256,128]{2,1,0:T(8,128)(2,1)S(1)}, u32[]{:S(2)}, u32[]{:S(2)}) collective-permute-start(bf16[4,256,128]{2,1,0:T(8,128)(2,1)S(1)} %get-tuple-element.21.own_ref), channel_id=1, source_target_pairs={{0,12},{4,0},{8,4},{12,8},{1,13},{5,1},{9,5},{13,9},{2,14},{6,2},{... | collective-permute-start | bytes 786440 | tf_op jit(solution)/shard_map/ppermute | solution.py:24
  116.9 13.2 %collective-permute-start.9 = (bf16[4,256,128]{2,1,0:T(8,128)(2,1)S(1)}, bf16[4,256,128]{2,1,0:T(8,128)(2,1)S(1)}, u32[]{:S(2)}, u32[]{:S(2)}) collective-permute-start(bf16[4,256,128]{2,1,0:T(8,128)(2,1)S(1)} %get-tuple-element.21.own_ref), channel_id=1, source_target_pairs={{0,8},{4,12},{8,0},{12,4},{1,9},{5,13},{9,1},{13,5},{2,10},{6,14},... | collective-permute-start | bytes 786440 | tf_op jit(solution)/shard_map/ppermute | solution.py:24
  134.8 12.1 %all-to-all-start.4 = ((f32[16,4,128]{2,1,0:T(4,128)}), f32[16,4,128]{2,1,0:T(4,128)S(1)}, u32[]{:S(2)}, u32[]{:S(2)}) async-start(f32[16,4,128]{2,1,0:T(4,128)} %get-tuple-element.24), calls=%async_computation.4 | async-start | bytes 65536 | tf_op jit(solution)/shard_map/all_to_all | solution.py:28
  (7 other events, 14.5 us)
